TPU v7x, 256 devices: a whole 4x4x8 slice. The times are simulated.
256 devices in a mesh: ep: 16 (over y, x), tp: 16 (over z, core).
Axes of the slice: x: 4, y: 4, z: 8, core: 2. Of those that a mesh axis runs over, the one named last changes fastest.
Arguments:
- tokens: bfloat16 [256, 4096], P('ep'), may hold values from -150 to 150
- query_weight: bfloat16 [4096, 1024], P('tp'), may hold values from -0.09375 to 0.09375
- key_weight: bfloat16 [4096, 1024], P('tp'), may hold values from -0.09375 to 0.09375
- value_weight: bfloat16 [4096, 2048], P(None, 'tp'), may hold values from -0.09375 to 0.09375
- decay_down: bfloat16 [4096, 16], replicated, may hold values from -0.09375 to 0.09375
- decay_up: float32 [16, 1024], replicated, may hold values from -3 to 3
- decay_bias: float32 [1024], replicated, may hold values from -8 to 4
- old_state: float32 [256, 256, 2048], P('ep', None, 'tp'), may hold values from -8 to 8
- out_weight: bfloat16 [2048, 4096], P('tp'), may hold values from -0.1875 to 0.1875
- norm_gain: float32 [4096], replicated, may hold values from 0.2 to 4
- router_weight: bfloat16 [4096, 16], replicated, may hold values from -0.09375 to 0.09375
- routing: int32 [256, 2], P('ep'), may hold values from 0 to 15, all different within a row; in each aligned block of 16 rows (0 to 15, 16 to 31, ...) at most 4 rows name the same one
- glu_weight: bfloat16 [16, 4096, 2048], P('ep', None, 'tp'), may hold values from -0.25 to 0.25
- linear_weight: bfloat16 [16, 4096, 2048], P('ep', None, 'tp'), may hold values from -0.25 to 0.25
- down_weight: bfloat16 [16, 2048, 4096], P('ep', 'tp'), may hold values from -0.01953125 to 0.01953125
- final_gain: float32 [4096], replicated, may hold values from 0.1 to 1.9
Outputs:
- layer_out: bfloat16 [256, 4096], P('ep', 'tp')
- new_state: float32 [256, 256, 2048], P('ep', None, 'tp')
Inputs may be any that keep to these rules, and one draw needn't show every extreme that they name: `routing`: within the rows of one device (aligned blocks of 16 rows) no expert is named by more than 4 rows, and at least one block reaches that bound; each row names 2 different experts.
All inputs are finite; a program needn't handle non-finite values.
Results may differ from a plain program's by a relative error of at most 0.015.
Values may be sent and summed in bfloat16 or wider, within the bound.
A program may use at most 64 MiB of HBM per device.

v0:
```python
import jax
import jax.numpy as jnp
from jax import lax
from jax.sharding import Mesh
from jax.sharding import PartitionSpec as P

TP = ("tp_0", "tp_1")


ALPHA = 2.0**0.25
TAU = 16.0
LIMIT = 7.0
SLOPE = 1.702
EPSILON = 1e-05


def filled_up(lines, length):
    spare = -lines.shape[0] % length
    if not spare:
        return lines
    return jnp.concatenate([lines, jnp.zeros((spare, *lines.shape[1:]), lines.dtype)])


def laid_out(blocks, dim):
    lengths = list(blocks.shape[1:])
    lengths[dim] *= blocks.shape[0]
    return jnp.moveaxis(blocks, 0, dim).reshape(lengths)


def copy_for_each(shard, axis):
    copies = jnp.broadcast_to(shard, (lax.axis_size(axis), *shard.shape))
    return lax.all_to_all(copies, axis, split_axis=0, concat_axis=0, tiled=True)


def gather_directly(shard, axis, dim):
    return laid_out(copy_for_each(shard, axis), dim)


def cut_along(shard, dim, length):
    before, after = (shard.shape[:dim], shard.shape[dim + 1 :])
    return jnp.moveaxis(shard.reshape(*before, length, -1, *after), dim, 0)


def sent_and_summed(shard, axis, dim):
    blocks = cut_along(shard, dim, lax.axis_size(axis))
    arrived = lax.all_to_all(blocks, axis, split_axis=0, concat_axis=0, tiled=True)
    return arrived.sum(axis=0)


def sum_by_parts(shard, axes):
    padded = filled_up(shard, lax.axis_size(axes))
    whole = gather_directly(sent_and_summed(padded, axes, 0), axes, 0)
    return lax.slice_in_dim(whole, 0, len(shard)).reshape(shard.shape)


def packed_total(arrays, axis):
    flat, at, outs = (jnp.concatenate([a.reshape(-1) for a in arrays]), 0, [])
    subtotal = sum_by_parts(flat, axis)
    for a in arrays:
        outs.append(subtotal[at : at + a.size].reshape(a.shape))
        at += a.size
    return tuple(outs)


def sum_at_owner(shard, axis, dim):
    blocks = cut_along(shard, dim, lax.axis_size(axis))
    arrived = lax.all_to_all(blocks, axis, split_axis=0, concat_axis=0, tiled=True)
    return arrived.astype(jnp.float32).sum(axis=0)


def sum_in_two_steps(shard, axes, dim):
    far, near = axes
    own = sum_at_owner(cut_along(shard, dim, lax.axis_size(far)), near, dim + 1)
    return jnp.sum(
        lax.all_to_all(own.astype(jnp.bfloat16), far, 0, 0, tiled=True).astype(jnp.float32), axis=0
    )


def gathered_by_axis(shard, axes, dim):
    far, near = axes
    leading = copy_for_each(shard, far)
    blocks = jnp.swapaxes(copy_for_each(leading, near), 0, 1)
    return laid_out(blocks.reshape(-1, *shard.shape), dim)


def nested_sum(shard, axes):
    lines = shard.reshape(-1, shard.shape[-1])
    own = sum_in_two_steps(
        filled_up(lines, lax.axis_size(axes[0]) * lax.axis_size(axes[1])), axes, 0
    )
    whole = gathered_by_axis(own.astype(jnp.bfloat16), axes, 0)
    return whole[: len(lines)].reshape(shard.shape).astype(jnp.float32)


def nested_sum_2(shard, axes):
    lines = shard.reshape(-1, shard.shape[-1])
    padded = filled_up(lines, lax.axis_size(axes))
    whole = gather_directly(sent_and_summed(padded, axes, 0), axes, 0)
    return lax.slice_in_dim(whole, 0, len(lines)).reshape(shard.shape)


def layer_norm(inputs, gain):
    mean = jnp.mean(inputs, axis=-1, keepdims=True)
    centered = inputs - mean
    variance = jnp.mean(centered * centered, axis=-1, keepdims=True)
    return centered * lax.rsqrt(variance + EPSILON) * gain


def clamped_unit(glu_pre, linear_pre):
    glu = jnp.minimum(glu_pre, LIMIT)
    linear = jnp.clip(linear_pre, -LIMIT, LIMIT)
    return glu * jax.nn.sigmoid(SLOPE * glu) * (linear + 1.0)


def expert_gate(logits, slot_ids, own_expert):
    expert_ids = jnp.arange(logits.shape[1], dtype=jnp.int32)
    picked = jnp.sum(
        jnp.where(slot_ids[:, :, None] == expert_ids[None, None, :], logits[:, None, :], 0.0),
        axis=2,
    )
    own_logit = jnp.sum(jnp.where(expert_ids[None, :] == own_expert, logits, 0.0), axis=1)
    return jnp.exp(own_logit) / jnp.sum(jnp.exp(picked), axis=1)


def per_device(
    tokens,
    query_weight,
    key_weight,
    value_weight,
    decay_down,
    decay_up,
    decay_bias,
    old_state,
    out_weight,
    norm_gain,
    router_weight,
    routing,
    glu_weight,
    linear_weight,
    down_weight,
    final_gain,
):
    tp_count = lax.axis_size(TP)
    tp_rank = lax.axis_index(TP)
    own_expert = lax.axis_index("ep")
    seq_count, width = tokens.shape
    head_dk = old_state.shape[1]
    heads = query_weight.shape[1] // head_dk
    head_start = tp_rank // (tp_count // heads) * head_dk
    top_count = routing.shape[1]
    experts = router_weight.shape[1]
    slot_cap = max(2, (2 * seq_count * top_count + experts - 1) // experts)
    share_width = width // tp_count
    share_start = tp_rank * share_width
    glu_local = glu_weight[0]
    linear_local = linear_weight[0]
    down_local = down_weight[0]
    token_share = lax.dynamic_slice_in_dim(tokens, share_start, share_width, 1)
    query_part = jnp.dot(token_share, query_weight, preferred_element_type=jnp.float32)
    key_part = jnp.dot(token_share, key_weight, preferred_element_type=jnp.float32)
    query_sum, key_sum = packed_total((query_part, key_part), TP)
    query_all = query_sum.astype(jnp.bfloat16)
    key_all = key_sum.astype(jnp.bfloat16)
    values = jnp.dot(tokens, value_weight, preferred_element_type=jnp.float32).astype(jnp.bfloat16)
    low_rank = jnp.dot(tokens, decay_down, preferred_element_type=jnp.float32)
    up_cols = lax.dynamic_slice_in_dim(decay_up, head_start, head_dk, 1)
    bias_cols = lax.dynamic_slice_in_dim(decay_bias, head_start, head_dk, 0)
    decay = jnp.exp(
        jax.nn.log_sigmoid(jnp.dot(low_rank, up_cols, precision=lax.Precision.HIGHEST) + bias_cols)
        / TAU
    )
    query = lax.dynamic_slice_in_dim(query_all, head_start, head_dk, 1).astype(jnp.float32)
    keys = lax.dynamic_slice_in_dim(key_all, head_start, head_dk, 1).astype(jnp.float32)
    new_state = (
        decay[:, :, None] * old_state + keys[:, :, None] * values.astype(jnp.float32)[:, None, :]
    )
    mixed = (
        jnp.einsum("si,sic->sc", query, new_state, precision=lax.Precision.HIGHEST)
        * head_dk ** (-0.5)
    ).astype(jnp.bfloat16)
    out_terms = jnp.dot(mixed, out_weight, preferred_element_type=jnp.float32)
    flat_ids = routing.reshape(-1)
    expert_ids = jnp.arange(experts, dtype=jnp.int32)
    chosen = (flat_ids[:, None] == expert_ids[None, :]).astype(jnp.int32)
    before = jnp.cumsum(chosen, axis=0) - chosen
    slot_rank = jnp.sum(before * chosen, axis=1)
    slot_index = flat_ids * slot_cap + slot_rank
    placed = (
        slot_index[:, None] == jnp.arange(experts * slot_cap, dtype=jnp.int32)[None, :]
    ).astype(jnp.int32)
    spread = jnp.sum(placed.reshape(seq_count, top_count, experts * slot_cap), axis=1)
    spread_rows = spread.astype(jnp.bfloat16)
    slot_ids = jnp.einsum("sn,sk->nk", spread, routing).reshape(experts, slot_cap, top_count)
    hidden_in = ALPHA * tokens.astype(jnp.float32) + nested_sum_2(out_terms, TP)
    normed = layer_norm(hidden_in, norm_gain).astype(jnp.bfloat16)
    send_rows = jnp.einsum(
        "sn,sd->nd", spread_rows, normed, preferred_element_type=jnp.float32
    ).astype(jnp.bfloat16)
    send_rows = send_rows.reshape(experts, slot_cap, normed.shape[1])
    rows_in = lax.all_to_all(send_rows, "ep", split_axis=0, concat_axis=0, tiled=True)
    ids_in = lax.all_to_all(slot_ids, "ep", split_axis=0, concat_axis=0, tiled=True)
    sources, slots, row_width = rows_in.shape
    flat = rows_in.reshape(sources * slots, row_width)
    act = clamped_unit(
        jnp.dot(flat, glu_local, preferred_element_type=jnp.float32),
        jnp.dot(flat, linear_local, preferred_element_type=jnp.float32),
    ).astype(jnp.bfloat16)
    summed = nested_sum(
        jnp.dot(act, down_local, preferred_element_type=jnp.float32).astype(jnp.bfloat16),
        ("tp_0", "tp_1"),
    )
    logits = jnp.dot(flat, router_weight, preferred_element_type=jnp.float32)
    gate = expert_gate(logits, ids_in.reshape(sources * slots, top_count), own_expert)
    weighted = (summed * gate[:, None]).astype(jnp.bfloat16).reshape(sources, slots, row_width)
    returned = lax.all_to_all(weighted, "ep", split_axis=0, concat_axis=0, tiled=True)
    combined = ALPHA * normed.astype(jnp.float32) + jnp.einsum(
        "sn,nd->sd",
        spread_rows,
        returned.reshape(experts * slot_cap, normed.shape[1]),
        preferred_element_type=jnp.float32,
    )
    layer_out = lax.dynamic_slice_in_dim(
        layer_norm(combined, final_gain), share_start, share_width, 1
    ).astype(jnp.bfloat16)
    return (layer_out, new_state)


def solution(mesh):
    finer = Mesh(mesh.devices.reshape(mesh.shape["ep"], 8, 2), ("ep", "tp_0", "tp_1"))
    in_specs = (
        P("ep", None),
        P(TP, None),
        P(TP, None),
        P(None, TP),
        P(),
        P(),
        P(),
        P("ep", None, TP),
        P(TP, None),
        P(),
        P(),
        P("ep", None),
        P("ep", None, TP),
        P("ep", None, TP),
        P("ep", TP, None),
        P(),
    )
    out_specs = (P("ep", TP), P("ep", None, TP))
    return jax.shard_map(
        per_device, mesh=finer, in_specs=in_specs, out_specs=out_specs, check_vma=False
    )
```

profile of v0, /device:TPU:1, one launch (start us, length us, event | category | flops | bytes accessed | tf_op | source)
XLA Modules:
  0.0 162.4 jit_solution(6192603075886763918)
XLA Ops:
  0.7 1.4 fusion.34
  2.1 1.4 fusion.32
  3.5 0.7 all_to_all.37
  4.3 10.0 %all-to-all-start = ((f32[16,1,2048]{2,1,0:T(1,128)}), f32[16,1,2048]{2,1,0:T(1,128)S(1)}, u32[]{:S(2)}, u32[]{:S(2)}) async-start(f32[16,1,2048]{2,1,0:T(1,128)} %all_to_all.37), calls=%async_computation | async-start | bytes 262144 | tf_op jit(solution)/shard_map/all_to_all | solution.py:46
  14.2 1.1 fusion.49
  15.3 0.8 dynamic_slice.21
  16.1 1.5 fusion.4
  17.6 5.6 %all-to-all-done = f32[16,1,2048]{2,1,0:T(1,128)S(1)} async-done(((f32[16,1,2048]{2,1,0:T(1,128)}), f32[16,1,2048]{2,1,0:T(1,128)S(1)}, u32[]{:S(2)}, u32[]{:S(2)}) %all-to-all-start) | async-done | bytes 131104 | tf_op jit(solution)/shard_map/all_to_all | solution.py:46
  23.3 0.5 broadcast.105
  23.8 1.0 reduce.8
  24.8 0.7 reshape.136
  25.5 3.4 %all-to-all-start.1 = ((bf16[16,2,1024]{2,1,0:T(2,128)(2,1)}), bf16[16,2,1024]{2,1,0:T(2,128)(2,1)S(1)}, u32[]{:S(2)}, u32[]{:S(2)}) async-start(bf16[16,2,1024]{2,1,0:T(2,128)(2,1)} %reshape.136), calls=%async_computation.1 | async-start | bytes 131072 | tf_op jit(solution)/shard_map/all_to_all | solution.py:32
  28.9 0.9 fusion.21
  29.8 6.6 %all-to-all-done.1 = bf16[16,2,1024]{2,1,0:T(2,128)(2,1)S(1)} async-done(((bf16[16,2,1024]{2,1,0:T(2,128)(2,1)}), bf16[16,2,1024]{2,1,0:T(2,128)(2,1)S(1)}, u32[]{:S(2)}, u32[]{:S(2)}) %all-to-all-start.1) | async-done | bytes 65568 | tf_op jit(solution)/shard_map/all_to_all | solution.py:32
  36.8 1.2 multiply_add_fusion
  38.0 1.3 copy-done.1
  39.4 0.8 fusion.24
  40.1 0.4 copy-done.5
  40.8 1.0 copy.87
  41.8 3.6 %all-to-all-start.2 = ((f32[16,1,4096]{2,1,0:T(1,128)}), f32[16,1,4096]{2,1,0:T(1,128)S(1)}, u32[]{:S(2)}, u32[]{:S(2)}) async-start(f32[16,1,4096]{2,1,0:T(1,128)} %copy.87), calls=%async_computation.2 | async-start | bytes 524288 | tf_op jit(solution)/shard_map/all_to_all | solution.py:46
  45.5 11.6 %all-to-all-done.2 = f32[16,1,4096]{2,1,0:T(1,128)S(1)} async-done(((f32[16,1,4096]{2,1,0:T(1,128)}), f32[16,1,4096]{2,1,0:T(1,128)S(1)}, u32[]{:S(2)}, u32[]{:S(2)}) %all-to-all-start.2) | async-done | bytes 262176 | tf_op jit(solution)/shard_map/all_to_all | solution.py:46
  57.3 0.9 broadcast_in_dim.33
  58.2 3.4 %all-to-all-start.3 = ((f32[16,1,4096]{2,1,0:T(1,128)}), f32[16,1,4096]{2,1,0:T(1,128)S(1)}, u32[]{:S(2)}, u32[]{:S(2)}) async-start(f32[16,1,4096]{2,1,0:T(1,128)} %broadcast_in_dim.33), calls=%async_computation.3 | async-start | bytes 524288 | tf_op jit(solution)/shard_map/all_to_all | solution.py:32
  62.2 10.4 %all-to-all-done.3 = f32[16,1,4096]{2,1,0:T(1,128)S(1)} async-done(((f32[16,1,4096]{2,1,0:T(1,128)}), f32[16,1,4096]{2,1,0:T(1,128)S(1)}, u32[]{:S(2)}, u32[]{:S(2)}) %all-to-all-start.3) | async-done | bytes 262176 | tf_op jit(solution)/shard_map/all_to_all | solution.py:32
  73.3 0.3 convolution_convert_fusion.1
  73.6 1.0 reshape.127
  74.6 6.9 %all-to-all-start.4 = ((bf16[16,4,4096]{2,1,0:T(4,128)(2,1)}), bf16[16,4,4096]{2,1,0:T(4,128)(2,1)S(1)}, u32[]{:S(2)}, u32[]{:S(2)}) async-start(bf16[16,4,4096]{2,1,0:T(4,128)(2,1)} %reshape.127), calls=%async_computation.4 | async-start | bytes 1048576 | tf_op jit(solution)/shard_map/all_to_all | solution.py:200
  81.6 0.5 fusion.11
  82.1 0.7 copy.95
  82.8 9.8 %all-to-all-done.4 = bf16[16,4,4096]{2,1,0:T(4,128)(2,1)S(1)} async-done(((bf16[16,4,4096]{2,1,0:T(4,128)(2,1)}), bf16[16,4,4096]{2,1,0:T(4,128)(2,1)S(1)}, u32[]{:S(2)}, u32[]{:S(2)}) %all-to-all-start.4) | async-done | bytes 524320 | tf_op jit(solution)/shard_map/all_to_all | solution.py:200
  92.8 1.5 convolution_minimum_fusion
  94.3 0.6 convolution_convert_fusion
  95.3 5.2 %all_to_all.60 = bf16[2,8,4,4096]{3,2,1,0:T(4,128)(2,1)S(1)} all-to-all(bf16[2,8,4,4096]{3,2,1,0:T(4,128)(2,1)S(1)} %bitcast.55), channel_id=1, replica_groups=mesh['ep'=16,'tp_0'=8,'tp_1'=2] {'tp_1'}, dimensions={0} | all-to-all | bytes 1048576 | tf_op jit(solution)/shard_map/all_to_all | solution.py:67
  100.5 3.5 %all-to-all-start.9 = ((s32[16,4,2]{1,2,0:T(2,128)}), s32[16,4,2]{1,2,0:T(2,128)S(1)}, u32[]{:S(2)}, u32[]{:S(2)}) async-start(s32[16,4,2]{1,2,0:T(2,128)} %copy.95), calls=%async_computation.9 | async-start | bytes 32768 | tf_op jit(solution)/shard_map/all_to_all | solution.py:201
  104.0 1.2 reduce_sum.132
  105.2 5.2 %all-to-all-done.9 = s32[16,4,2]{1,2,0:T(2,128)S(1)} async-done(((s32[16,4,2]{1,2,0:T(2,128)}), s32[16,4,2]{1,2,0:T(2,128)S(1)}, u32[]{:S(2)}, u32[]{:S(2)}) %all-to-all-start.9) | async-done | bytes 544 | tf_op jit(solution)/shard_map/all_to_all | solution.py:201
  110.4 3.4 %all-to-all-start.6 = ((bf16[8,4,4096]{2,1,0:T(4,128)(2,1)}), bf16[8,4,4096]{2,1,0:T(4,128)(2,1)S(1)}, u32[]{:S(2)}, u32[]{:S(2)}) async-start(bf16[8,4,4096]{2,1,0:T(4,128)(2,1)} %reduce_sum.132), calls=%async_computation.6 | async-start | bytes 524288 | tf_op jit(solution)/shard_map/all_to_all | solution.py:75
  113.9 10.0 %all-to-all-done.6 = bf16[8,4,4096]{2,1,0:T(4,128)(2,1)S(1)} async-done(((bf16[8,4,4096]{2,1,0:T(4,128)(2,1)}), bf16[8,4,4096]{2,1,0:T(4,128)(2,1)S(1)}, u32[]{:S(2)}, u32[]{:S(2)}) %all-to-all-start.6) | async-done | bytes 262176 | tf_op jit(solution)/shard_map/all_to_all | solution.py:75
  124.0 0.8 broadcast_in_dim.34
  124.8 3.4 %all-to-all-start.7 = ((bf16[8,4,4096]{2,1,0:T(4,128)(2,1)}), bf16[8,4,4096]{2,1,0:T(4,128)(2,1)S(1)}, u32[]{:S(2)}, u32[]{:S(2)}) async-start(bf16[8,4,4096]{2,1,0:T(4,128)(2,1)} %broadcast_in_dim.34), calls=%async_computation.7 | async-start | bytes 524288 | tf_op jit(solution)/shard_map/all_to_all | solution.py:32
  128.6 8.9 %all-to-all-done.7 = bf16[8,4,4096]{2,1,0:T(4,128)(2,1)S(1)} async-done(((bf16[8,4,4096]{2,1,0:T(4,128)(2,1)}), bf16[8,4,4096]{2,1,0:T(4,128)(2,1)S(1)}, u32[]{:S(2)}, u32[]{:S(2)}) %all-to-all-start.7) | async-done | bytes 262176 | tf_op jit(solution)/shard_map/all_to_all | solution.py:32
  137.7 7.5 %all_to_all.61 = bf16[2,8,4,4096]{3,2,1,0:T(4,128)(2,1)S(1)} all-to-all(bf16[2,8,4,4096]{3,2,1,0:T(4,128)(2,1)S(1)} %broadcast_in_dim.35), channel_id=1, replica_groups=mesh['ep'=16,'tp_0'=8,'tp_1'=2] {'tp_1'}, dimensions={0} | all-to-all | bytes 1048576 | tf_op jit(solution)/shard_map/all_to_all | solution.py:32
  145.4 1.1 fusion.5
  146.5 3.6 %all-to-all-start.10 = ((bf16[16,4,4096]{2,1,0:T(4,128)(2,1)}), bf16[16,4,4096]{2,1,0:T(4,128)(2,1)S(1)}, u32[]{:S(2)}, u32[]{:S(2)}) async-start(bf16[16,4,4096]{2,1,0:T(4,128)(2,1)} %fusion.5), calls=%async_computation.10 | async-start | bytes 1048576 | tf_op jit(solution)/shard_map/all_to_all | solution.py:215
  150.1 0.8 dynamic-slice
  150.9 10.2 %all-to-all-done.10 = bf16[16,4,4096]{2,1,0:T(4,128)(2,1)S(1)} async-done(((bf16[16,4,4096]{2,1,0:T(4,128)(2,1)}), bf16[16,4,4096]{2,1,0:T(4,128)(2,1)S(1)}, u32[]{:S(2)}, u32[]{:S(2)}) %all-to-all-start.10) | async-done | bytes 524320 | tf_op jit(solution)/shard_map/all_to_all | solution.py:215
  161.1 0.3 fusion.48
  161.7 0.7 fusion.23
  (63 shorter events, 4.5 us)
Async XLA Ops:
  0.6 93.7 %copy-start = (bf16[1,128,4096]{2,1,0:T(8,128)(2,1)S(1)}, bf16[1,128,4096]{2,1,0:T(8,128)(2,1)}, u32[]{:S(2)}) copy-start(bf16[1,128,4096]{2,1,0:T(8,128)(2,1)} %param.30) | copy-start | bytes 3145732
  0.6 13.6 %copy-start.2 = (bf16[16,4096]{1,0:T(8,128)(2,1)S(1)}, bf16[16,4096]{1,0:T(8,128)(2,1)}, u32[]{:S(2)}) copy-start(bf16[16,4096]{1,0:T(8,128)(2,1)} %param.16) | copy-start | bytes 393220
  2.1 34.7 %copy-start.3 = (f32[16,256,128]{2,1,0:T(8,128)S(1)}, f32[16,256,128]{2,1,0:T(8,128)}, u32[]{:S(2)}) copy-start(f32[16,256,128]{2,1,0:T(8,128)} %param.23) | copy-start | bytes 6291460
  4.3 18.9 %all-to-all-start = ((f32[16,1,2048]{2,1,0:T(1,128)}), f32[16,1,2048]{2,1,0:T(1,128)S(1)}, u32[]{:S(2)}, u32[]{:S(2)}) async-start(f32[16,1,2048]{2,1,0:T(1,128)} %all_to_all.37), calls=%async_computation | async-start | bytes 262144 | tf_op jit(solution)/shard_map/all_to_all | solution.py:46
  25.5 10.9 %all-to-all-start.1 = ((bf16[16,2,1024]{2,1,0:T(2,128)(2,1)}), bf16[16,2,1024]{2,1,0:T(2,128)(2,1)S(1)}, u32[]{:S(2)}, u32[]{:S(2)}) async-start(bf16[16,2,1024]{2,1,0:T(2,128)(2,1)} %reshape.136), calls=%async_computation.1 | async-start | bytes 131072 | tf_op jit(solution)/shard_map/all_to_all | solution.py:32
  38.0 1.3 copy-start.1
  39.4 1.2 copy-start.5
  39.4 6.0 %copy-start.8 = (s32[16,2]{0,1:T(2,128)S(1)}, s32[16,2]{0,1:T(2,128)}, u32[]{:S(2)}) copy-start(s32[16,2]{0,1:T(2,128)} %param.27) | copy-start | bytes 388
  40.6 32.6 %copy-start.7 = (f32[4096]{0:T(1024)S(1)}, f32[4096]{0:T(1024)}, u32[]{:S(2)}) copy-start(f32[4096]{0:T(1024)} %param.25) | copy-start | bytes 49156
  41.8 15.3 %all-to-all-start.2 = ((f32[16,1,4096]{2,1,0:T(1,128)}), f32[16,1,4096]{2,1,0:T(1,128)S(1)}, u32[]{:S(2)}, u32[]{:S(2)}) async-start(f32[16,1,4096]{2,1,0:T(1,128)} %copy.87), calls=%async_computation.2 | async-start | bytes 524288 | tf_op jit(solution)/shard_map/all_to_all | solution.py:46
  58.2 14.4 %all-to-all-start.3 = ((f32[16,1,4096]{2,1,0:T(1,128)}), f32[16,1,4096]{2,1,0:T(1,128)S(1)}, u32[]{:S(2)}, u32[]{:S(2)}) async-start(f32[16,1,4096]{2,1,0:T(1,128)} %broadcast_in_dim.33), calls=%async_computation.3 | async-start | bytes 524288 | tf_op jit(solution)/shard_map/all_to_all | solution.py:32
  74.6 19.7 %copy-start.4 = (bf16[1,4096,128]{2,1,0:T(8,128)(2,1)S(1)}, bf16[1,4096,128]{2,1,0:T(8,128)(2,1)}, u32[]{:S(2)}) copy-start(bf16[1,4096,128]{2,1,0:T(8,128)(2,1)} %param.29) | copy-start | bytes 3145732
  74.6 18.0 %all-to-all-start.4 = ((bf16[16,4,4096]{2,1,0:T(4,128)(2,1)}), bf16[16,4,4096]{2,1,0:T(4,128)(2,1)S(1)}, u32[]{:S(2)}, u32[]{:S(2)}) async-start(bf16[16,4,4096]{2,1,0:T(4,128)(2,1)} %reshape.127), calls=%async_computation.4 | async-start | bytes 1048576 | tf_op jit(solution)/shard_map/all_to_all | solution.py:200
  95.1 33.1 %copy-start.6 = (bf16[4096,16]{0,1:T(8,128)(2,1)S(1)}, bf16[4096,16]{0,1:T(8,128)(2,1)}, u32[]{:S(2)}) copy-start(bf16[4096,16]{0,1:T(8,128)(2,1)} %param.26) | copy-start | bytes 393220
  100.5 9.9 %all-to-all-start.9 = ((s32[16,4,2]{1,2,0:T(2,128)}), s32[16,4,2]{1,2,0:T(2,128)S(1)}, u32[]{:S(2)}, u32[]{:S(2)}) async-start(s32[16,4,2]{1,2,0:T(2,128)} %copy.95), calls=%async_computation.9 | async-start | bytes 32768 | tf_op jit(solution)/shard_map/all_to_all | solution.py:201
  110.4 13.5 %all-to-all-start.6 = ((bf16[8,4,4096]{2,1,0:T(4,128)(2,1)}), bf16[8,4,4096]{2,1,0:T(4,128)(2,1)S(1)}, u32[]{:S(2)}, u32[]{:S(2)}) async-start(bf16[8,4,4096]{2,1,0:T(4,128)(2,1)} %reduce_sum.132), calls=%async_computation.6 | async-start | bytes 524288 | tf_op jit(solution)/shard_map/all_to_all | solution.py:75
  124.8 12.7 %all-to-all-start.7 = ((bf16[8,4,4096]{2,1,0:T(4,128)(2,1)}), bf16[8,4,4096]{2,1,0:T(4,128)(2,1)S(1)}, u32[]{:S(2)}, u32[]{:S(2)}) async-start(bf16[8,4,4096]{2,1,0:T(4,128)(2,1)} %broadcast_in_dim.34), calls=%async_computation.7 | async-start | bytes 524288 | tf_op jit(solution)/shard_map/all_to_all | solution.py:32
  146.5 14.5 %all-to-all-start.10 = ((bf16[16,4,4096]{2,1,0:T(4,128)(2,1)}), bf16[16,4,4096]{2,1,0:T(4,128)(2,1)S(1)}, u32[]{:S(2)}, u32[]{:S(2)}) async-start(bf16[16,4,4096]{2,1,0:T(4,128)(2,1)} %fusion.5), calls=%async_computation.10 | async-start | bytes 1048576 | tf_op jit(solution)/shard_map/all_to_all | solution.py:215
where the time goes:
time: 164 us; the launch traced here: 162 us
  waiting for transfers between devices  78.1 us (48%)
  starting transfers between devices  41.1 us (25%)
  blocking collectives  12.7 us (8%)
  local copies, waits for them, and re-layouts  11.6 us (7%)
  matrix products  10.7 us (7%)
  other arithmetic  7.17 us (4%)
    all_to_all x3, waiting for transfers between devices, copy_for_each(): return lax.all_to_all(copies, axis, split_axis=0, concat_axis=0, tiled=True)  25.8 us
    all_to_all x2, waiting for transfers between devices, sent_and_summed(): lax.all_to_all(blocks, axis, split_axis=0, concat_axis=0, tiled=True)  17.1 us
    all_to_all x2, starting transfers between devices, sent_and_summed(): lax.all_to_all(blocks, axis, split_axis=0, concat_axis=0, tiled=True)  13.5 us
    all_to_all x3, starting transfers between devices, copy_for_each(): return lax.all_to_all(copies, axis, split_axis=0, concat_axis=0, tiled=True)  10.2 us
    all_to_all x1, waiting for transfers between devices, per_device(): lax.all_to_all(weighted, 'ep', split_axis=0, concat_axis=0, tiled=True)  10.2 us
    all_to_all x1, waiting for transfers between devices, sum_in_two_steps(): lax.all_to_all(own.astype(jnp.bfloat16), far, 0, 0, tiled=True)  9.99 us
    all_to_all x1, waiting for transfers between devices, per_device(): lax.all_to_all(send_rows, 'ep', split_axis=0, concat_axis=0, tiled=True)  9.83 us
    all_to_all x1, blocking collectives, copy_for_each(): return lax.all_to_all(copies, axis, split_axis=0, concat_axis=0, tiled=True)  7.51 us
  transfers between devices with their start and end apart: 9, of which 9 were waited for; matrix products, arithmetic and copies ran while one was open for 5% of the time, Pallas kernels for 0%

commit v1 on v0

v1 whole, which is shorter than its diff:
```python
import functools

import jax
import jax.numpy as jnp
from jax import lax
from jax.experimental import pallas as pl
from jax.experimental.pallas import tpu as pltpu
from jax.sharding import PartitionSpec as P

ALPHA = 2.0**0.25
TAU = 16.0
LIMIT = 7.0
SLOPE = 1.702
EPSILON = 1e-05
MESH = pl.DeviceIdType.MESH
F32 = jnp.float32
BF16 = jnp.bfloat16

N = 16
ROWS = 16
D = 4096
PIECE = 256
HALF = 2048
CAP = 4
KEYS = 256
LANES = 128


def dot(a, b):
    return jnp.dot(a, b, preferred_element_type=F32)


def dot_nt(a, b, precision=None):
    return lax.dot_general(a, b, (((1,), (1,)), ((), ())), precision=precision, preferred_element_type=F32)


def iota(shape, dim):
    return lax.broadcasted_iota(jnp.int32, shape, dim)


def remote(src, dst, send_sem, recv_sem, **where):
    return pltpu.make_async_remote_copy(
        src_ref=src, dst_ref=dst, send_sem=send_sem, recv_sem=recv_sem, device_id=where, device_id_type=MESH
    )


def kernel(
    tok_h, qw_h, kw_h, vw_h, dd_h, du_h, db_h, st_h, ow_h, ng_h, rw_h, rt_h, glu_h, lin_h, dn_h, fg_h,
    out_ref, ns_h,
    tok, qw, kw, vw, dd, du, db, st, ow, ng, rw, rt, gl, dn, fg, ns,
    sq, rq, rqk, mixed, sp, rp, rg, h, nrm, sd, rd, rd2, xs, sh, rh, sr, rr, sm, rm, ss, rs,
    loc, s1, r1, s1b, r1b, s2, r2, s3, r3, s4, r4, s4d, r4d, s5, r5, s6, r6, s7, r7, s8, r8,
):
    e = lax.axis_index("ep")
    t = lax.axis_index("tp")
    z = t // 2
    c = lax.rem(t, 2)
    head = t // 4
    member = lax.rem(t, 4)
    partner = t + 1 - 2 * c

    def around(base, step, size):
        return lax.rem(base + step, size)

    head_cols = pl.ds(pl.multiple_of(head * KEYS, KEYS), KEYS)
    fetches = [
        (tok_h, tok), (qw_h, qw), (kw_h, kw), (dd_h, dd), (du_h.at[:, head_cols], du), (db_h.at[:, head_cols], db),
        (vw_h, vw), (st_h, st), (ow_h, ow), (ng_h, ng), (rw_h, rw), (rt_h, rt),
        (glu_h.at[0], gl.at[:, pl.ds(0, LANES)]), (lin_h.at[0], gl.at[:, pl.ds(LANES, LANES)]),
        (dn_h.at[0], dn), (fg_h.at[:, pl.ds(pl.multiple_of(t * PIECE, PIECE), PIECE)], fg),
    ]
    copies = [pltpu.make_async_copy(a, b, loc.at[i]) for i, (a, b) in enumerate(fetches)]
    for copy in copies:
        copy.start()

    def fetched(*which):
        for i in which:
            copies[i].wait()

    barrier = pltpu.get_barrier_semaphore()
    for step in range(1, N):
        pl.semaphore_signal(barrier, inc=1, device_id={"tp": around(t, step, N)}, device_id_type=MESH)
        pl.semaphore_signal(barrier, inc=1, device_id={"ep": around(e, step, N)}, device_id_type=MESH)

    fetched(0, 1, 2)
    share = tok[:, pl.ds(pl.multiple_of(t * PIECE, PIECE), PIECE)]
    q_part = dot(share, qw[...]).astype(BF16)
    k_part = dot(share, kw[...]).astype(BF16)
    for i in range(N):
        part = q_part if i % 4 < 2 else k_part
        at = (i // 4) * KEYS + (i % 2) * LANES
        sq[i] = part[:, at : at + LANES]
    pl.semaphore_wait(barrier, 2 * (N - 1))
    sends = []

    def send(*args, **where):
        copy = remote(*args, **where)
        copy.start()
        sends.append(copy)

    for step in range(1, N):
        to = around(t, step, N)
        send(sq.at[to], rq.at[t], s1.at[to], r1.at[t], tp=to)
    rq[t] = sq[t]

    fetched(3, 4, 5, 6)
    tokens = tok[...]
    values = dot(tokens, vw[...]).astype(BF16)
    low_rank = dot_nt(tokens, dd[...])
    pre = jnp.dot(low_rank, du[...], precision=lax.Precision.HIGHEST, preferred_element_type=F32) + db[...]
    log_sig = -(jnp.maximum(-pre, 0.0) + jnp.log1p(jnp.exp(-jnp.abs(pre))))
    decay = jnp.exp(log_sig / TAU)
    hi = decay.astype(BF16)
    rest = decay - hi.astype(F32)
    mid = rest.astype(BF16)
    low = (rest - mid.astype(F32)).astype(BF16)
    thirds = jnp.concatenate([hi.astype(F32), mid.astype(F32), low.astype(F32)], axis=0)
    wide = ROWS * LANES
    ones3 = (lax.rem(iota((3 * ROWS, wide), 0), ROWS) == iota((3 * ROWS, wide), 1) // LANES).astype(BF16)
    decay_wide = dot(jnp.transpose(thirds).astype(BF16), ones3)
    fetched(7)
    for s in range(ROWS):
        ns[s] = decay_wide[:, s * LANES : (s + 1) * LANES] * st[s]
    own_block = iota((ROWS, wide), 0) == iota((ROWS, wide), 1) // LANES
    ones1 = own_block.astype(BF16)
    values_f = values.astype(F32)
    values_wide = jnp.where(own_block, jnp.concatenate([values_f] * ROWS, axis=1), 0.0).astype(BF16)

    def received(recv, sems, step, base, size, axis):
        src = around(base, step, size)
        remote(recv.at[src], recv.at[src], s1.at[0], sems.at[src], **{axis: src}).wait_recv()

    for step in range(1, N):
        received(rq, r1, step, t, N, "tp")
    rqk[member] = jnp.sum(rq[...].astype(F32), axis=0).astype(BF16)
    for step in range(1, 4):
        to = around(member, step, 4)
        send(rqk.at[member], rqk.at[member], s1b.at[to], r1b.at[member], tp=head * 4 + to)
    for step in range(1, 4):
        src = around(member, step, 4)
        remote(rqk.at[src], rqk.at[src], s1b.at[0], r1b.at[src], tp=head * 4 + src).wait_recv()

    query = jnp.concatenate([rqk[0], rqk[1]], axis=1).astype(F32)
    keys = jnp.concatenate([rqk[2], rqk[3]], axis=1).astype(F32)
    update = dot(jnp.transpose(keys).astype(BF16), values_wide)
    query_wide = dot(jnp.transpose(query).astype(BF16), ones1)
    for s in range(ROWS):
        cols = slice(s * LANES, (s + 1) * LANES)
        new = ns[s] + update[:, cols]
        ns[s] = new
        mixed[s : s + 1, :] = jnp.sum(query_wide[:, cols] * new, axis=0, keepdims=True)
    state_out = pltpu.make_async_copy(ns, ns_h, loc.at[16])
    state_out.start()

    fetched(8)
    attn_part = dot((mixed[...] * KEYS ** (-0.5)).astype(BF16), ow[...]).astype(BF16)
    for i in range(N):
        sp[i] = attn_part[:, i * PIECE : (i + 1) * PIECE]
    for step in range(1, N):
        to = around(t, step, N)
        send(sp.at[to], rp.at[t], s2.at[to], r2.at[t], tp=to)
    rp[t] = sp[t]

    fetched(9, 10, 11)
    slots = N * CAP
    routed = rt[...]
    ids = iota((N, ROWS), 0)
    chosen = ((routed[0:1, :] == ids) | (routed[1:2, :] == ids)).astype(F32)
    upper = (iota((ROWS, ROWS), 0) < iota((ROWS, ROWS), 1)).astype(BF16)
    rank = dot(chosen.astype(BF16), upper)
    expand = (iota((slots, N), 0) // CAP == iota((slots, N), 1)).astype(BF16)
    here = dot(expand, chosen.astype(BF16)) > 0.5
    place = dot(expand, rank.astype(BF16))
    spread = (here & (place == lax.rem(iota((slots, ROWS), 0), CAP).astype(F32))).astype(F32)

    for step in range(1, N):
        received(rp, r2, step, t, N, "tp")
    rg[t] = jnp.sum(rp[...].astype(F32), axis=0).astype(BF16)
    for step in range(1, N):
        to = around(t, step, N)
        send(rg.at[t], rg.at[t], s3.at[to], r3.at[t], tp=to)
    for step in range(1, N):
        received(rg, r3, step, t, N, "tp")

    for i in range(N):
        cols = slice(i * PIECE, (i + 1) * PIECE)
        h[:, cols] = ALPHA * tok[:, cols].astype(F32) + rg[i].astype(F32)
    hidden = h[...]
    centred = hidden - jnp.mean(hidden, axis=1, keepdims=True)
    var = jnp.mean(centred * centred, axis=1, keepdims=True)
    nrm[...] = (centred * lax.rsqrt(var + EPSILON) * ng[...]).astype(BF16)

    def block(j, core):
        return pl.ds(pl.multiple_of((2 * j + core) * PIECE, PIECE), PIECE)

    half = jnp.concatenate([nrm[:, block(j, c)] for j in range(N // 2)], axis=1)
    packed = dot(spread.astype(BF16), half)
    for i in range(N):
        sd[i] = packed[i * CAP : (i + 1) * CAP].astype(BF16)
    for step in range(1, N):
        to = around(e, step, N)
        send(sd.at[to], rd.at[e], s4.at[to], r4.at[e], ep=to)
    send(sd.at[e], rd2.at[e], s4d.at[e], r4d.at[e], tp=partner)
    rd[e] = sd[e]

    logits = dot_nt(rw[...], nrm[...])
    raised = jnp.where(chosen > 0.5, jnp.exp(logits), 0.0)
    gates = raised / jnp.sum(raised, axis=0, keepdims=True)
    gate_rows = spread * jnp.dot(
        expand.astype(F32), gates, precision=lax.Precision.HIGHEST, preferred_element_type=F32
    )
    gate_cols = jnp.transpose(gate_rows)
    gate_hi = gate_cols.astype(BF16)
    gate_lo = (gate_cols - gate_hi.astype(F32)).astype(BF16)

    for step in range(1, N):
        received(rd, r4, step, e, N, "ep")
        src = around(e, step, N)
        send(rd.at[src], rd2.at[src], s4d.at[src], r4d.at[src], tp=partner)
    fetched(12, 13)
    for i in range(N):
        xs[i * CAP : (i + 1) * CAP, :] = rd[i].astype(F32)
    rows = xs[...].astype(BF16)
    pre_act = sum(dot(rows[:, j * PIECE : (j + 1) * PIECE], gl[block(j, c), :]) for j in range(N // 2))
    for i in range(N):
        remote(rd2.at[i], rd2.at[i], s1.at[0], r4d.at[i], tp=partner).wait_recv()
    for i in range(N):
        xs[i * CAP : (i + 1) * CAP, :] = rd2[i].astype(F32)
    rows = xs[...].astype(BF16)
    pre_act += sum(dot(rows[:, j * PIECE : (j + 1) * PIECE], gl[block(j, 1 - c), :]) for j in range(N // 2))
    glu = jnp.minimum(pre_act[:, :LANES], LIMIT)
    linear = jnp.clip(pre_act[:, LANES:], -LIMIT, LIMIT)
    act = (glu * jax.nn.sigmoid(SLOPE * glu) * (linear + 1.0)).astype(BF16)

    fetched(14)
    for j in range(N // 2):
        sh[j] = dot(act, dn[:, block(j, 1 - c)]).astype(BF16)
        send(sh.at[j], rh.at[j], s5.at[j], r5.at[j], tp=partner)
    for j in range(N // 2):
        mine = dot(act, dn[:, block(j, c)])
        remote(rh.at[j], rh.at[j], s1.at[0], r5.at[j], tp=partner).wait_recv()
        total = (mine + rh[j].astype(F32)).astype(BF16)
        for i in range(N):
            sr[i, :, j * PIECE : (j + 1) * PIECE] = total[i * CAP : (i + 1) * CAP]
    for step in range(1, N):
        to = around(e, step, N)
        send(sr.at[to], rr.at[e], s6.at[to], r6.at[e], ep=to)
    rr[e] = sr[e]
    for step in range(1, N):
        received(rr, r6, step, e, N, "ep")

    for i in range(N):
        xs[i * CAP : (i + 1) * CAP, :] = rr[i].astype(F32)
    back = xs[...].astype(BF16)
    mix = (dot(gate_hi, back) + dot(gate_lo, back)).astype(BF16)
    for j in range(N // 2):
        sm[j] = mix[:, j * PIECE : (j + 1) * PIECE]
    for step in range(1, N // 2):
        to = around(z, step, N // 2)
        send(sm.at[to], rm.at[z], s7.at[to], r7.at[z], tp=2 * to + c)
    rm[z] = sm[z]
    for step in range(1, N // 2):
        src = around(z, step, N // 2)
        remote(rm.at[src], rm.at[src], s1.at[0], r7.at[src], tp=2 * src + c).wait_recv()
    own = nrm[:, pl.ds(pl.multiple_of(t * PIECE, PIECE), PIECE)].astype(F32)
    u = ALPHA * own + jnp.sum(rm[...].astype(F32), axis=0)

    part_mean = jnp.mean(u, axis=1, keepdims=True)
    part_sq = jnp.sum((u - part_mean) ** 2, axis=1, keepdims=True)
    lane, row = iota((ROWS, LANES), 1), iota((ROWS, LANES), 0)
    line = jnp.where(lane == row, part_mean, jnp.where(lane == row + ROWS, part_sq, 0.0))
    ss[...] = jnp.sum(line, axis=0, keepdims=True)
    for step in range(1, N):
        to = around(t, step, N)
        send(ss, rs.at[t], s8.at[to], r8.at[t], tp=to)
    rs[t] = ss[...]
    fetched(15)
    for step in range(1, N):
        received(rs, r8, step, t, N, "tp")
    means = jnp.concatenate([rs[i] for i in range(N)], axis=0)
    total = jnp.sum(means, axis=0, keepdims=True)
    spread_sq = jnp.sum((means - total / N) ** 2, axis=0, keepdims=True)
    mean = jnp.sum(jnp.where(lane == row, total / N, 0.0), axis=1, keepdims=True)
    between = jnp.sum(jnp.where(lane == row, spread_sq, 0.0), axis=1, keepdims=True)
    within = jnp.sum(jnp.where(lane == row + ROWS, total, 0.0), axis=1, keepdims=True)
    variance = (within + PIECE * between) / D
    out_ref[...] = ((u - mean) * lax.rsqrt(variance + EPSILON) * fg[...]).astype(BF16)

    state_out.wait()
    for copy in sends:
        copy.wait_send()


def step(
    tokens, query_weight, key_weight, value_weight, decay_down, decay_up, decay_bias, old_state, out_weight,
    norm_gain, router_weight, routing, glu_weight, linear_weight, down_weight, final_gain,
):
    hbm = pl.BlockSpec(memory_space=pl.ANY)
    vmem, dma = pltpu.VMEM, pltpu.SemaphoreType.DMA
    return pl.pallas_call(
        kernel,
        out_shape=(
            jax.ShapeDtypeStruct((ROWS, PIECE), BF16),
            jax.ShapeDtypeStruct(old_state.shape, F32),
        ),
        in_specs=[hbm] * 16,
        out_specs=(pl.BlockSpec(memory_space=pltpu.VMEM), hbm),
        scratch_shapes=[
            vmem((ROWS, D), BF16), vmem((PIECE, 1024), BF16), vmem((PIECE, 1024), BF16), vmem((D, LANES), BF16),
            vmem((N, D), BF16), vmem((16, KEYS), F32), vmem((1, KEYS), F32), vmem((ROWS, KEYS, LANES), F32),
            vmem((LANES, D), BF16), vmem((1, D), F32), vmem((N, D), BF16), vmem((2, ROWS), jnp.int32),
            vmem((D, 2 * LANES), BF16), vmem((LANES, D), BF16), vmem((1, PIECE), F32), vmem((ROWS, KEYS, LANES), F32),
            vmem((N, ROWS, LANES), BF16), vmem((N, ROWS, LANES), BF16), vmem((4, ROWS, LANES), BF16),
            vmem((ROWS, LANES), F32), vmem((N, ROWS, PIECE), BF16), vmem((N, ROWS, PIECE), BF16),
            vmem((N, ROWS, PIECE), BF16), vmem((ROWS, D), F32), vmem((ROWS, D), BF16),
            vmem((N, CAP, HALF), BF16), vmem((N, CAP, HALF), BF16), vmem((N, CAP, HALF), BF16),
            vmem((N * CAP, HALF), F32), vmem((N // 2, N * CAP, PIECE), BF16), vmem((N // 2, N * CAP, PIECE), BF16),
            vmem((N, CAP, HALF), BF16), vmem((N, CAP, HALF), BF16), vmem((N // 2, ROWS, PIECE), BF16),
            vmem((N // 2, ROWS, PIECE), BF16), vmem((1, LANES), F32), vmem((N, 1, LANES), F32),
            dma((17,)), dma((N,)), dma((N,)), dma((4,)), dma((4,)), dma((N,)), dma((N,)), dma((N,)), dma((N,)),
            dma((N,)), dma((N,)), dma((N,)), dma((N,)), dma((N // 2,)), dma((N // 2,)), dma((N,)), dma((N,)),
            dma((N // 2,)), dma((N // 2,)), dma((N,)), dma((N,)),
        ],
        compiler_params=pltpu.CompilerParams(
            collective_id=0, has_side_effects=True, vmem_limit_bytes=60 * 1024 * 1024
        ),
        name="decode_step",
    )(
        tokens, query_weight, key_weight, value_weight, decay_down.T, decay_up, decay_bias.reshape(1, -1), old_state,
        out_weight, norm_gain.reshape(1, -1), router_weight.T, routing.T, glu_weight, linear_weight, down_weight,
        final_gain.reshape(1, -1),
    )


def solution(mesh):
    in_specs = (
        P("ep", None), P("tp", None), P("tp", None), P(None, "tp"), P(), P(), P(), P("ep", None, "tp"), P("tp", None),
        P(), P(), P("ep", None), P("ep", None, "tp"), P("ep", None, "tp"), P("ep", "tp", None), P(),
    )
    out_specs = (P("ep", "tp"), P("ep", None, "tp"))
    return jax.shard_map(step, mesh=mesh, in_specs=in_specs, out_specs=out_specs, check_vma=False)
```

time: 164 us -> 66.6 us (0.41)
  waiting for transfers between devices: 78.1 us -> 0 us
  Pallas kernels: 0 us -> 61.4 us
  starting transfers between devices: 41.1 us -> 0 us
  blocking collectives: 12.7 us -> 0 us
  matrix products: 10.7 us -> 0 us
  local copies, waits for them, and re-layouts: 11.6 us -> 4.41 us
  other arithmetic: 7.17 us -> 0 us
    all_to_all x9 -> x0, waiting for transfers between devices: 78.1 us -> none  [the longest x3 25.8 us: copy_for_each(): return lax.all_to_all(copies, axis, split_axis=0, concat_axis=0, tiled=True)]
    pallas_call x0 -> x1, Pallas kernels: none -> 61.4 us  [step(): pl.pallas_call(kernel, out_shape=(jax.ShapeDtypeStruct((ROWS, PIECE), BF1...]
    all_to_all x9 -> x0, starting transfers between devices: 41.1 us -> none  [the longest x2 13.5 us: sent_and_summed(): lax.all_to_all(blocks, axis, split_axis=0, concat_axis=0, tiled=True)]
    all_to_all x2 -> x0, blocking collectives: 12.7 us -> none  [the longest x1 7.51 us: copy_for_each(): return lax.all_to_all(copies, axis, split_axis=0, concat_axis=0, tiled=True)]
    dot_general x13 -> x0, matrix products: 10.7 us -> none  [the longest x1 1.54 us: per_device(): jnp.dot(flat, glu_local, preferred_element_type=jnp.float32)]
    reduce_sum x11 -> x0, other arithmetic: 2.68 us -> none  [the longest x1 1.21 us: sum_at_owner(): return arrived.astype(jnp.float32).sum(axis=0)]
    broadcast_in_dim x5 -> x0, local copies, waits for them, and re-layouts: 2.44 us -> none  [copy_for_each(): copies = jnp.broadcast_to(shard, (lax.axis_size(axis), *shard.shape))]
    reshape x4 -> x0, local copies, waits for them, and re-layouts: 2.19 us -> none  [the longest x1 0.99 us: per_device(): send_rows = send_rows.reshape(experts, slot_cap, normed.shape[1])]
  transfers between devices with their start and end apart: 9 -> 0, of which waited for: 9 -> 0; matrix products, arithmetic and copies ran while one was open for 5% -> 0% of each run, Pallas kernels for 0% -> 0%
where the time goes in v1:
time: 66.6 us; the launch traced here: 66.4 us
  Pallas kernels  61.4 us (92%)
  local copies, waits for them, and re-layouts  4.41 us (7%)
    pallas_call x1, Pallas kernels, step(): pl.pallas_call(kernel, out_shape=(jax.ShapeDtypeStruct((ROWS, PIECE), BF1...  61.4 us
    unnamed x2, local copies, waits for them, and re-layouts  4.41 us

profile of v1, /device:TPU:1, one launch (start us, length us, event | category | flops | bytes accessed | tf_op | source)
XLA Modules:
  0.0 66.4 jit_solution(15532304077554560038)
XLA Ops:
  0.6 61.4 %decode_step.1 = (bf16[16,256]{1,0:T(8,128)(2,1)}, f32[16,256,128]{2,1,0:T(8,128)}) custom-call(bf16[16,4096]{1,0:T(8,128)(2,1)} %tok_h.1, bf16[256,1024]{1,0:T(8,128)(2,1)} %qw_h.1, bf16[256,1024]{1,0:T(8,128)(2,1)} %kw_h.1, bf16[4096,128]{1,0:T(8,128)(2,1)} %vw_h.1, bf16[16,4096]{1,0:T(8,128)(2,1)} %bitcast.6, f32[16,1024]{1,0:T(8,128)} %du_h.1, ...), custom_call_target="tpu_custom_call" | custom-call | tf_op jit(solution)/shard_map/decode_step/pallas_call | solution.py:300
  62.0 1.3 %copy.20 = bf16[16,256]{1,0:T(8,128)(2,1)} copy(bf16[16,256]{1,0:T(8,128)(2,1)} %get-tuple-element.4) | data formatting | bytes 16384
  63.3 3.1 %copy.21 = f32[16,256,128]{2,1,0:T(8,128)} copy(f32[16,256,128]{2,1,0:T(8,128)} %get-tuple-element.5) | data formatting | bytes 4194304

commit v2 on v1

--- a/solution.py
+++ b/solution.py
@@ -38,6 +38,17 @@
     return lax.broadcasted_iota(jnp.int32, shape, dim)
 
 
+_scopes = []
+
+
+def mark(name):
+    while _scopes:
+        _scopes.pop().__exit__(None, None, None)
+    if name:
+        _scopes.append(jax.named_scope(name))
+        _scopes[-1].__enter__()
+
+
 def remote(src, dst, send_sem, recv_sem, **where):
     return pltpu.make_async_remote_copy(
         src_ref=src, dst_ref=dst, send_sem=send_sem, recv_sem=recv_sem, device_id=where, device_id_type=MESH
@@ -46,10 +57,10 @@
 
 def kernel(
     tok_h, qw_h, kw_h, vw_h, dd_h, du_h, db_h, st_h, ow_h, ng_h, rw_h, rt_h, glu_h, lin_h, dn_h, fg_h,
-    out_ref, ns_h,
-    tok, qw, kw, vw, dd, du, db, st, ow, ng, rw, rt, gl, dn, fg, ns,
+    out_ref, ns,
+    tok, qw, kw, vw, dd, du, db, st, ow, ng, rw, rt, gl, dn, fg,
     sq, rq, rqk, mixed, sp, rp, rg, h, nrm, sd, rd, rd2, xs, sh, rh, sr, rr, sm, rm, ss, rs,
-    loc, s1, r1, s1b, r1b, s2, r2, s3, r3, s4, r4, s4d, r4d, s5, r5, s6, r6, s7, r7, s8, r8,
+    loc, out_sem, in_sem,
 ):
     e = lax.axis_index("ep")
     t = lax.axis_index("tp")
@@ -62,6 +73,7 @@
     def around(base, step, size):
         return lax.rem(base + step, size)
 
+    mark("fetch")
     head_cols = pl.ds(pl.multiple_of(head * KEYS, KEYS), KEYS)
     fetches = [
         (tok_h, tok), (qw_h, qw), (kw_h, kw), (dd_h, dd), (du_h.at[:, head_cols], du), (db_h.at[:, head_cols], db),
@@ -77,12 +89,15 @@
         for i in which:
             copies[i].wait()
 
+    mark("barrier_signal")
     barrier = pltpu.get_barrier_semaphore()
     for step in range(1, N):
         pl.semaphore_signal(barrier, inc=1, device_id={"tp": around(t, step, N)}, device_id_type=MESH)
         pl.semaphore_signal(barrier, inc=1, device_id={"ep": around(e, step, N)}, device_id_type=MESH)
 
+    mark("qk_fetch_wait")
     fetched(0, 1, 2)
+    mark("qk_dot")
     share = tok[:, pl.ds(pl.multiple_of(t * PIECE, PIECE), PIECE)]
     q_part = dot(share, qw[...]).astype(BF16)
     k_part = dot(share, kw[...]).astype(BF16)
@@ -90,19 +105,31 @@
         part = q_part if i % 4 < 2 else k_part
         at = (i // 4) * KEYS + (i % 2) * LANES
         sq[i] = part[:, at : at + LANES]
+    mark("barrier_wait")
     pl.semaphore_wait(barrier, 2 * (N - 1))
-    sends = []
-
-    def send(*args, **where):
-        copy = remote(*args, **where)
-        copy.start()
-        sends.append(copy)
+    mark("s1_send")
+    pending = []
+
+    def send(phase, src, dst, **where):
+        remote(src, dst, out_sem.at[phase], in_sem.at[phase], **where).start()
+
+    def sent(phase, like, count):
+        pending.append((phase, like, count))
+
+    def whole(phase, like, count):
+        ref = like if count is None else like.at[pl.ds(0, count)]
+        return remote(ref, ref, out_sem.at[phase], in_sem.at[phase], tp=partner)
+
+    def arrived(phase, like, count):
+        whole(phase, like, count).wait_recv()
 
     for step in range(1, N):
         to = around(t, step, N)
-        send(sq.at[to], rq.at[t], s1.at[to], r1.at[t], tp=to)
+        send(0, sq.at[to], rq.at[t], tp=to)
+    sent(0, sq, N - 1)
     rq[t] = sq[t]
 
+    mark("decay")
     fetched(3, 4, 5, 6)
     tokens = tok[...]
     values = dot(tokens, vw[...]).astype(BF16)
@@ -118,6 +145,7 @@
     wide = ROWS * LANES
     ones3 = (lax.rem(iota((3 * ROWS, wide), 0), ROWS) == iota((3 * ROWS, wide), 1) // LANES).astype(BF16)
     decay_wide = dot(jnp.transpose(thirds).astype(BF16), ones3)
+    mark("state_decay")
     fetched(7)
     for s in range(ROWS):
         ns[s] = decay_wide[:, s * LANES : (s + 1) * LANES] * st[s]
@@ -126,20 +154,17 @@
     values_f = values.astype(F32)
     values_wide = jnp.where(own_block, jnp.concatenate([values_f] * ROWS, axis=1), 0.0).astype(BF16)
 
-    def received(recv, sems, step, base, size, axis):
-        src = around(base, step, size)
-        remote(recv.at[src], recv.at[src], s1.at[0], sems.at[src], **{axis: src}).wait_recv()
-
-    for step in range(1, N):
-        received(rq, r1, step, t, N, "tp")
+    mark("r1_wait")
+    arrived(0, rq, N - 1)
+    mark("r1_sum_r1b")
     rqk[member] = jnp.sum(rq[...].astype(F32), axis=0).astype(BF16)
     for step in range(1, 4):
         to = around(member, step, 4)
-        send(rqk.at[member], rqk.at[member], s1b.at[to], r1b.at[member], tp=head * 4 + to)
-    for step in range(1, 4):
-        src = around(member, step, 4)
-        remote(rqk.at[src], rqk.at[src], s1b.at[0], r1b.at[src], tp=head * 4 + src).wait_recv()
-
+        send(1, rqk.at[member], rqk.at[member], tp=head * 4 + to)
+    sent(1, rqk, 3)
+    arrived(1, rqk, 3)
+
+    mark("state")
     query = jnp.concatenate([rqk[0], rqk[1]], axis=1).astype(F32)
     keys = jnp.concatenate([rqk[2], rqk[3]], axis=1).astype(F32)
     update = dot(jnp.transpose(keys).astype(BF16), values_wide)
@@ -149,18 +174,19 @@
         new = ns[s] + update[:, cols]
         ns[s] = new
         mixed[s : s + 1, :] = jnp.sum(query_wide[:, cols] * new, axis=0, keepdims=True)
-    state_out = pltpu.make_async_copy(ns, ns_h, loc.at[16])
-    state_out.start()
-
+
+    mark("out_dot_s2")
     fetched(8)
     attn_part = dot((mixed[...] * KEYS ** (-0.5)).astype(BF16), ow[...]).astype(BF16)
     for i in range(N):
         sp[i] = attn_part[:, i * PIECE : (i + 1) * PIECE]
     for step in range(1, N):
         to = around(t, step, N)
-        send(sp.at[to], rp.at[t], s2.at[to], r2.at[t], tp=to)
+        send(2, sp.at[to], rp.at[t], tp=to)
+    sent(2, sp, N - 1)
     rp[t] = sp[t]
 
+    mark("slots")
     fetched(9, 10, 11)
     slots = N * CAP
     routed = rt[...]
@@ -173,15 +199,18 @@
     place = dot(expand, rank.astype(BF16))
     spread = (here & (place == lax.rem(iota((slots, ROWS), 0), CAP).astype(F32))).astype(F32)
 
-    for step in range(1, N):
-        received(rp, r2, step, t, N, "tp")
+    mark("r2_wait")
+    arrived(2, rp, N - 1)
+    mark("s3_send")
     rg[t] = jnp.sum(rp[...].astype(F32), axis=0).astype(BF16)
     for step in range(1, N):
         to = around(t, step, N)
-        send(rg.at[t], rg.at[t], s3.at[to], r3.at[t], tp=to)
-    for step in range(1, N):
-        received(rg, r3, step, t, N, "tp")
-
+        send(3, rg.at[t], rg.at[t], tp=to)
+    sent(3, rg, N - 1)
+    mark("r3_wait")
+    arrived(3, rg, N - 1)
+
+    mark("norm1")
     for i in range(N):
         cols = slice(i * PIECE, (i + 1) * PIECE)
         h[:, cols] = ALPHA * tok[:, cols].astype(F32) + rg[i].astype(F32)
@@ -193,16 +222,20 @@
     def block(j, core):
         return pl.ds(pl.multiple_of((2 * j + core) * PIECE, PIECE), PIECE)
 
+    mark("s4_send")
     half = jnp.concatenate([nrm[:, block(j, c)] for j in range(N // 2)], axis=1)
     packed = dot(spread.astype(BF16), half)
     for i in range(N):
         sd[i] = packed[i * CAP : (i + 1) * CAP].astype(BF16)
     for step in range(1, N):
         to = around(e, step, N)
-        send(sd.at[to], rd.at[e], s4.at[to], r4.at[e], ep=to)
-    send(sd.at[e], rd2.at[e], s4d.at[e], r4d.at[e], tp=partner)
+        send(4, sd.at[to], rd.at[e], ep=to)
+    sent(4, sd, N - 1)
+    send(5, sd.at[e], rd2.at[e], tp=partner)
+    sent(5, sd, 1)
     rd[e] = sd[e]
 
+    mark("gates")
     logits = dot_nt(rw[...], nrm[...])
     raised = jnp.where(chosen > 0.5, jnp.exp(logits), 0.0)
     gates = raised / jnp.sum(raised, axis=0, keepdims=True)
@@ -213,17 +246,22 @@
     gate_hi = gate_cols.astype(BF16)
     gate_lo = (gate_cols - gate_hi.astype(F32)).astype(BF16)
 
-    for step in range(1, N):
-        received(rd, r4, step, e, N, "ep")
+    mark("r4_wait_fwd")
+    arrived(4, rd, N - 1)
+    for step in range(1, N):
         src = around(e, step, N)
-        send(rd.at[src], rd2.at[src], s4d.at[src], r4d.at[src], tp=partner)
+        send(6, rd.at[src], rd2.at[src], tp=partner)
+    sent(6, rd, N - 1)
+    mark("up_own")
     fetched(12, 13)
     for i in range(N):
         xs[i * CAP : (i + 1) * CAP, :] = rd[i].astype(F32)
     rows = xs[...].astype(BF16)
     pre_act = sum(dot(rows[:, j * PIECE : (j + 1) * PIECE], gl[block(j, c), :]) for j in range(N // 2))
-    for i in range(N):
-        remote(rd2.at[i], rd2.at[i], s1.at[0], r4d.at[i], tp=partner).wait_recv()
+    mark("r4d_wait")
+    arrived(5, rd2, 1)
+    arrived(6, rd2, N - 1)
+    mark("up_other")
     for i in range(N):
         xs[i * CAP : (i + 1) * CAP, :] = rd2[i].astype(F32)
     rows = xs[...].astype(BF16)
@@ -232,23 +270,30 @@
     linear = jnp.clip(pre_act[:, LANES:], -LIMIT, LIMIT)
     act = (glu * jax.nn.sigmoid(SLOPE * glu) * (linear + 1.0)).astype(BF16)
 
+    mark("down")
     fetched(14)
     for j in range(N // 2):
         sh[j] = dot(act, dn[:, block(j, 1 - c)]).astype(BF16)
-        send(sh.at[j], rh.at[j], s5.at[j], r5.at[j], tp=partner)
+        send(7, sh.at[j], rh.at[j], tp=partner)
+    sent(7, sh, None)
+    mine = [dot(act, dn[:, block(j, c)]) for j in range(N // 2)]
+    mark("down_wait")
+    arrived(7, rh, None)
+    mark("down_sum")
     for j in range(N // 2):
-        mine = dot(act, dn[:, block(j, c)])
-        remote(rh.at[j], rh.at[j], s1.at[0], r5.at[j], tp=partner).wait_recv()
-        total = (mine + rh[j].astype(F32)).astype(BF16)
+        total = (mine[j] + rh[j].astype(F32)).astype(BF16)
         for i in range(N):
             sr[i, :, j * PIECE : (j + 1) * PIECE] = total[i * CAP : (i + 1) * CAP]
+    mark("s6_send")
     for step in range(1, N):
         to = around(e, step, N)
-        send(sr.at[to], rr.at[e], s6.at[to], r6.at[e], ep=to)
+        send(8, sr.at[to], rr.at[e], ep=to)
+    sent(8, sr, N - 1)
     rr[e] = sr[e]
-    for step in range(1, N):
-        received(rr, r6, step, e, N, "ep")
-
+    mark("r6_wait")
+    arrived(8, rr, N - 1)
+
+    mark("mix_s7")
     for i in range(N):
         xs[i * CAP : (i + 1) * CAP, :] = rr[i].astype(F32)
     back = xs[...].astype(BF16)
@@ -257,11 +302,12 @@
         sm[j] = mix[:, j * PIECE : (j + 1) * PIECE]
     for step in range(1, N // 2):
         to = around(z, step, N // 2)
-        send(sm.at[to], rm.at[z], s7.at[to], r7.at[z], tp=2 * to + c)
+        send(9, sm.at[to], rm.at[z], tp=2 * to + c)
+    sent(9, sm, N // 2 - 1)
     rm[z] = sm[z]
-    for step in range(1, N // 2):
-        src = around(z, step, N // 2)
-        remote(rm.at[src], rm.at[src], s1.at[0], r7.at[src], tp=2 * src + c).wait_recv()
+    mark("r7_wait")
+    arrived(9, rm, N // 2 - 1)
+    mark("stats_s8")
     own = nrm[:, pl.ds(pl.multiple_of(t * PIECE, PIECE), PIECE)].astype(F32)
     u = ALPHA * own + jnp.sum(rm[...].astype(F32), axis=0)
 
@@ -272,11 +318,13 @@
     ss[...] = jnp.sum(line, axis=0, keepdims=True)
     for step in range(1, N):
         to = around(t, step, N)
-        send(ss, rs.at[t], s8.at[to], r8.at[t], tp=to)
+        send(10, ss, rs.at[t], tp=to)
+    sent(10, rs, N - 1)
     rs[t] = ss[...]
+    mark("r8_wait")
     fetched(15)
-    for step in range(1, N):
-        received(rs, r8, step, t, N, "tp")
+    arrived(10, rs, N - 1)
+    mark("final")
     means = jnp.concatenate([rs[i] for i in range(N)], axis=0)
     total = jnp.sum(means, axis=0, keepdims=True)
     spread_sq = jnp.sum((means - total / N) ** 2, axis=0, keepdims=True)
@@ -286,9 +334,10 @@
     variance = (within + PIECE * between) / D
     out_ref[...] = ((u - mean) * lax.rsqrt(variance + EPSILON) * fg[...]).astype(BF16)
 
-    state_out.wait()
-    for copy in sends:
-        copy.wait_send()
+    mark("drain")
+    for phase, like, count in pending:
+        whole(phase, like, count).wait_send()
+    mark(None)
 
 
 def step(
@@ -300,16 +349,16 @@
     return pl.pallas_call(
         kernel,
         out_shape=(
-            jax.ShapeDtypeStruct((ROWS, PIECE), BF16),
-            jax.ShapeDtypeStruct(old_state.shape, F32),
+            pltpu.VMEM((ROWS, PIECE), BF16),
+            pltpu.VMEM(old_state.shape, F32),
         ),
         in_specs=[hbm] * 16,
-        out_specs=(pl.BlockSpec(memory_space=pltpu.VMEM), hbm),
+        out_specs=(pl.BlockSpec(memory_space=pltpu.VMEM), pl.BlockSpec(memory_space=pltpu.VMEM)),
         scratch_shapes=[
             vmem((ROWS, D), BF16), vmem((PIECE, 1024), BF16), vmem((PIECE, 1024), BF16), vmem((D, LANES), BF16),
             vmem((N, D), BF16), vmem((16, KEYS), F32), vmem((1, KEYS), F32), vmem((ROWS, KEYS, LANES), F32),
             vmem((LANES, D), BF16), vmem((1, D), F32), vmem((N, D), BF16), vmem((2, ROWS), jnp.int32),
-            vmem((D, 2 * LANES), BF16), vmem((LANES, D), BF16), vmem((1, PIECE), F32), vmem((ROWS, KEYS, LANES), F32),
+            vmem((D, 2 * LANES), BF16), vmem((LANES, D), BF16), vmem((1, PIECE), F32),
             vmem((N, ROWS, LANES), BF16), vmem((N, ROWS, LANES), BF16), vmem((4, ROWS, LANES), BF16),
             vmem((ROWS, LANES), F32), vmem((N, ROWS, PIECE), BF16), vmem((N, ROWS, PIECE), BF16),
             vmem((N, ROWS, PIECE), BF16), vmem((ROWS, D), F32), vmem((ROWS, D), BF16),
@@ -317,9 +366,7 @@
             vmem((N * CAP, HALF), F32), vmem((N // 2, N * CAP, PIECE), BF16), vmem((N // 2, N * CAP, PIECE), BF16),
             vmem((N, CAP, HALF), BF16), vmem((N, CAP, HALF), BF16), vmem((N // 2, ROWS, PIECE), BF16),
             vmem((N // 2, ROWS, PIECE), BF16), vmem((1, LANES), F32), vmem((N, 1, LANES), F32),
-            dma((17,)), dma((N,)), dma((N,)), dma((4,)), dma((4,)), dma((N,)), dma((N,)), dma((N,)), dma((N,)),
-            dma((N,)), dma((N,)), dma((N,)), dma((N,)), dma((N // 2,)), dma((N // 2,)), dma((N,)), dma((N,)),
-            dma((N // 2,)), dma((N // 2,)), dma((N,)), dma((N,)),
+            dma((16,)), dma((11,)), dma((11,)),
         ],
         compiler_params=pltpu.CompilerParams(
             collective_id=0, has_side_effects=True, vmem_limit_bytes=60 * 1024 * 1024

time: 66.6 us -> 60.8 us (0.913)
  Pallas kernels: 61.4 us -> 58.2 us
  local copies, waits for them, and re-layouts: 4.41 us -> 1.92 us
    pallas_call x1, Pallas kernels: 61.4 us -> 58.2 us  [step(): pl.pallas_call(kernel, out_shape=(pltpu.VMEM((ROWS, PIECE), BF16), pltpu....]
    unnamed x2, local copies, waits for them, and re-layouts: 4.41 us -> 1.92 us
where the time goes in v2:
time: 60.8 us; the launch traced here: 60.7 us
  Pallas kernels  58.2 us (96%)
  local copies, waits for them, and re-layouts  1.92 us (3%)
  between operations  0.65 us (1%)
    pallas_call x1, Pallas kernels, step(): pl.pallas_call(kernel, out_shape=(pltpu.VMEM((ROWS, PIECE), BF16), pltpu....  58.2 us
    unnamed x2, local copies, waits for them, and re-layouts  1.92 us

profile of v2, /device:TPU:1, one launch (start us, length us, event | category | flops | bytes accessed | tf_op | source)
XLA Modules:
  0.0 60.7 jit_solution(1991199870598986795)
XLA Ops:
  0.6 58.2 %decode_step.1 = (bf16[16,256]{1,0:T(8,128)(2,1)S(1)}, f32[16,256,128]{2,1,0:T(8,128)S(1)}) custom-call(bf16[16,4096]{1,0:T(8,128)(2,1)} %tok_h.1, bf16[256,1024]{1,0:T(8,128)(2,1)} %qw_h.1, bf16[256,1024]{1,0:T(8,128)(2,1)} %kw_h.1, bf16[4096,128]{1,0:T(8,128)(2,1)} %vw_h.1, bf16[16,4096]{1,0:T(8,128)(2,1)} %bitcast.6, f32[16,1024]{1,0:T(8,128)} %du_h.1, ...), custom_call_target="tpu_custom_call" | custom-call | tf_op jit(solution)/shard_map/decode_step/pallas_call | solution.py:349
  58.8 0.6 copy.20
  59.4 1.3 %copy.21 = f32[16,256,128]{2,1,0:T(8,128)} copy(f32[16,256,128]{2,1,0:T(8,128)S(1)} %get-tuple-element.3) | data formatting | bytes 4194304

commit v3 on v2

--- a/solution.py
+++ b/solution.py
@@ -24,6 +24,12 @@
 CAP = 4
 KEYS = 256
 LANES = 128
+FAR = (4, 3, 5, 2, 6, 1, 7)
+ALL_TP = [(d, x) for d in FAR for x in (1, 0)] + [(0, 1)]
+ALL_EP = sorted(
+    [(dy, dx) for dy in range(4) for dx in range(4) if dy or dx],
+    key=lambda p: -sum(min(d, 4 - d) for d in p),
+)
 
 
 def dot(a, b):
@@ -55,11 +61,34 @@
     )
 
 
+def diagonal(offset):
+    return iota((ROWS, LANES), 1) == iota((ROWS, LANES), 0) + offset
+
+
+def moments(part):
+    mean = jnp.mean(part, axis=1, keepdims=True)
+    squares = jnp.sum((part - mean) ** 2, axis=1, keepdims=True)
+    line = jnp.where(diagonal(0), mean, jnp.where(diagonal(ROWS), squares, 0.0))
+    return jnp.sum(line, axis=0, keepdims=True)
+
+
+def merged(lines):
+    lines = jnp.concatenate([lines[i] for i in range(N)], axis=0)
+    total = jnp.sum(lines, axis=0, keepdims=True)
+    apart = jnp.sum((lines - total / N) ** 2, axis=0, keepdims=True)
+
+    def column(line, offset):
+        return jnp.sum(jnp.where(diagonal(offset), line, 0.0), axis=1, keepdims=True)
+
+    variance = (column(total, ROWS) + PIECE * column(apart, 0)) / D
+    return column(total / N, 0), lax.rsqrt(variance + EPSILON)
+
+
 def kernel(
     tok_h, qw_h, kw_h, vw_h, dd_h, du_h, db_h, st_h, ow_h, ng_h, rw_h, rt_h, glu_h, lin_h, dn_h, fg_h,
     out_ref, ns,
     tok, qw, kw, vw, dd, du, db, st, ow, ng, rw, rt, gl, dn, fg,
-    sq, rq, rqk, mixed, sp, rp, rg, h, nrm, sd, rd, rd2, xs, sh, rh, sr, rr, sm, rm, ss, rs,
+    sq, rq, rqk, mixed, sp, rp, rg, nrm, sd, rd, rd2, xs, sh, rh, sr, rr, sm, rm, ss, rs, lg,
     loc, out_sem, in_sem,
 ):
     e = lax.axis_index("ep")
@@ -67,11 +96,13 @@
     z = t // 2
     c = lax.rem(t, 2)
     head = t // 4
-    member = lax.rem(t, 4)
     partner = t + 1 - 2 * c
 
-    def around(base, step, size):
-        return lax.rem(base + step, size)
+    def tp_at(d, x):
+        return 2 * lax.rem(z + d, N // 2) + lax.rem(c + x, 2)
+
+    def ep_at(dy, dx):
+        return 4 * lax.rem(e // 4 + dy, 4) + lax.rem(lax.rem(e, 4) + dx, 4)
 
     mark("fetch")
     head_cols = pl.ds(pl.multiple_of(head * KEYS, KEYS), KEYS)
@@ -91,9 +122,10 @@
 
     mark("barrier_signal")
     barrier = pltpu.get_barrier_semaphore()
-    for step in range(1, N):
-        pl.semaphore_signal(barrier, inc=1, device_id={"tp": around(t, step, N)}, device_id_type=MESH)
-        pl.semaphore_signal(barrier, inc=1, device_id={"ep": around(e, step, N)}, device_id_type=MESH)
+    for p in ALL_TP:
+        pl.semaphore_signal(barrier, inc=1, device_id={"tp": tp_at(*p)}, device_id_type=MESH)
+    for p in ALL_EP:
+        pl.semaphore_signal(barrier, inc=1, device_id={"ep": ep_at(*p)}, device_id_type=MESH)
 
     mark("qk_fetch_wait")
     fetched(0, 1, 2)
@@ -101,10 +133,10 @@
     share = tok[:, pl.ds(pl.multiple_of(t * PIECE, PIECE), PIECE)]
     q_part = dot(share, qw[...]).astype(BF16)
     k_part = dot(share, kw[...]).astype(BF16)
-    for i in range(N):
-        part = q_part if i % 4 < 2 else k_part
-        at = (i // 4) * KEYS + (i % 2) * LANES
-        sq[i] = part[:, at : at + LANES]
+    for i in range(4):
+        cols = slice(i * KEYS, (i + 1) * KEYS)
+        sq[0, i] = q_part[:, cols]
+        sq[1, i] = k_part[:, cols]
     mark("barrier_wait")
     pl.semaphore_wait(barrier, 2 * (N - 1))
     mark("s1_send")
@@ -123,11 +155,11 @@
     def arrived(phase, like, count):
         whole(phase, like, count).wait_recv()
 
-    for step in range(1, N):
-        to = around(t, step, N)
-        send(0, sq.at[to], rq.at[t], tp=to)
-    sent(0, sq, N - 1)
-    rq[t] = sq[t]
+    for d, x in ALL_TP:
+        to = tp_at(d, x)
+        send(0, sq.at[lax.rem(to, 2), to // 4], rq.at[t], tp=to)
+    sent(0, rq, N - 1)
+    rq[t] = sq[c, head]
 
     mark("decay")
     fetched(3, 4, 5, 6)
@@ -157,16 +189,12 @@
     mark("r1_wait")
     arrived(0, rq, N - 1)
     mark("r1_sum_r1b")
-    rqk[member] = jnp.sum(rq[...].astype(F32), axis=0).astype(BF16)
-    for step in range(1, 4):
-        to = around(member, step, 4)
-        send(1, rqk.at[member], rqk.at[member], tp=head * 4 + to)
-    sent(1, rqk, 3)
-    arrived(1, rqk, 3)
-
+    rqk[c] = jnp.sum(rq[...].astype(F32), axis=0).astype(BF16)
+    send(1, rqk.at[c], rqk.at[c], tp=partner)
+    sent(1, rqk, 1)
+    arrived(1, rqk, 1)
     mark("state")
-    query = jnp.concatenate([rqk[0], rqk[1]], axis=1).astype(F32)
-    keys = jnp.concatenate([rqk[2], rqk[3]], axis=1).astype(F32)
+    query, keys = rqk[0].astype(F32), rqk[1].astype(F32)
     update = dot(jnp.transpose(keys).astype(BF16), values_wide)
     query_wide = dot(jnp.transpose(query).astype(BF16), ones1)
     for s in range(ROWS):
@@ -180,8 +208,8 @@
     attn_part = dot((mixed[...] * KEYS ** (-0.5)).astype(BF16), ow[...]).astype(BF16)
     for i in range(N):
         sp[i] = attn_part[:, i * PIECE : (i + 1) * PIECE]
-    for step in range(1, N):
-        to = around(t, step, N)
+    for p in ALL_TP:
+        to = tp_at(*p)
         send(2, sp.at[to], rp.at[t], tp=to)
     sent(2, sp, N - 1)
     rp[t] = sp[t]
@@ -202,33 +230,35 @@
     mark("r2_wait")
     arrived(2, rp, N - 1)
     mark("s3_send")
-    rg[t] = jnp.sum(rp[...].astype(F32), axis=0).astype(BF16)
-    for step in range(1, N):
-        to = around(t, step, N)
-        send(3, rg.at[t], rg.at[t], tp=to)
-    sent(3, rg, N - 1)
+    rg[z] = jnp.sum(rp[...].astype(F32), axis=0).astype(BF16)
+    own_cols = pl.ds(pl.multiple_of(t * PIECE, PIECE), PIECE)
+    ss[0] = moments(ALPHA * tok[:, own_cols].astype(F32) + rg[z].astype(F32))
+    for d in FAR:
+        send(3, rg.at[z], rg.at[z], tp=tp_at(d, 0))
+    for p in ALL_TP:
+        send(11, ss.at[0], rs.at[0, t], tp=tp_at(*p))
+    rs[0, t] = ss[0]
+    sent(3, rg, N // 2 - 1)
+    sent(11, rs.at[0], N - 1)
     mark("r3_wait")
-    arrived(3, rg, N - 1)
+    arrived(11, rs.at[0], N - 1)
+    mean, scale = merged(rs[0])
+    arrived(3, rg, N // 2 - 1)
 
     mark("norm1")
-    for i in range(N):
-        cols = slice(i * PIECE, (i + 1) * PIECE)
-        h[:, cols] = ALPHA * tok[:, cols].astype(F32) + rg[i].astype(F32)
-    hidden = h[...]
-    centred = hidden - jnp.mean(hidden, axis=1, keepdims=True)
-    var = jnp.mean(centred * centred, axis=1, keepdims=True)
-    nrm[...] = (centred * lax.rsqrt(var + EPSILON) * ng[...]).astype(BF16)
-
     def block(j, core):
         return pl.ds(pl.multiple_of((2 * j + core) * PIECE, PIECE), PIECE)
 
+    for j in range(N // 2):
+        hidden = ALPHA * tok[:, block(j, c)].astype(F32) + rg[j].astype(F32)
+        nrm[:, j * PIECE : (j + 1) * PIECE] = ((hidden - mean) * scale * ng[:, block(j, c)]).astype(BF16)
+
     mark("s4_send")
-    half = jnp.concatenate([nrm[:, block(j, c)] for j in range(N // 2)], axis=1)
-    packed = dot(spread.astype(BF16), half)
+    packed = dot(spread.astype(BF16), nrm[...])
     for i in range(N):
         sd[i] = packed[i * CAP : (i + 1) * CAP].astype(BF16)
-    for step in range(1, N):
-        to = around(e, step, N)
+    for p in ALL_EP:
+        to = ep_at(*p)
         send(4, sd.at[to], rd.at[e], ep=to)
     sent(4, sd, N - 1)
     send(5, sd.at[e], rd2.at[e], tp=partner)
@@ -236,20 +266,16 @@
     rd[e] = sd[e]
 
     mark("gates")
-    logits = dot_nt(rw[...], nrm[...])
-    raised = jnp.where(chosen > 0.5, jnp.exp(logits), 0.0)
-    gates = raised / jnp.sum(raised, axis=0, keepdims=True)
-    gate_rows = spread * jnp.dot(
-        expand.astype(F32), gates, precision=lax.Precision.HIGHEST, preferred_element_type=F32
-    )
-    gate_cols = jnp.transpose(gate_rows)
-    gate_hi = gate_cols.astype(BF16)
-    gate_lo = (gate_cols - gate_hi.astype(F32)).astype(BF16)
+    rw_half = jnp.concatenate([rw[:, block(j, c)] for j in range(N // 2)], axis=1)
+    logit_part = dot_nt(rw_half, nrm[...])
+    lg[c] = jnp.concatenate([logit_part, jnp.zeros((N, LANES - ROWS), F32)], axis=1)
+    send(12, lg.at[c], lg.at[c], tp=partner)
+    sent(12, lg, 1)
 
     mark("r4_wait_fwd")
     arrived(4, rd, N - 1)
-    for step in range(1, N):
-        src = around(e, step, N)
+    for p in ALL_EP:
+        src = ep_at(*p)
         send(6, rd.at[src], rd2.at[src], tp=partner)
     sent(6, rd, N - 1)
     mark("up_own")
@@ -272,9 +298,10 @@
 
     mark("down")
     fetched(14)
+    theirs = [dot(act, dn[:, block(j, 1 - c)]) for j in range(N // 2)]
     for j in range(N // 2):
-        sh[j] = dot(act, dn[:, block(j, 1 - c)]).astype(BF16)
-        send(7, sh.at[j], rh.at[j], tp=partner)
+        sh[j] = theirs[j].astype(BF16)
+    send(7, sh, rh, tp=partner)
     sent(7, sh, None)
     mine = [dot(act, dn[:, block(j, c)]) for j in range(N // 2)]
     mark("down_wait")
@@ -285,11 +312,23 @@
         for i in range(N):
             sr[i, :, j * PIECE : (j + 1) * PIECE] = total[i * CAP : (i + 1) * CAP]
     mark("s6_send")
-    for step in range(1, N):
-        to = around(e, step, N)
+    for p in ALL_EP:
+        to = ep_at(*p)
         send(8, sr.at[to], rr.at[e], ep=to)
     sent(8, sr, N - 1)
     rr[e] = sr[e]
+    mark("gates2")
+    arrived(12, lg, 1)
+    logits = (lg[0] + lg[1])[:, :ROWS]
+    raised = jnp.where(chosen > 0.5, jnp.exp(logits), 0.0)
+    gates = raised / jnp.sum(raised, axis=0, keepdims=True)
+    gate_rows = spread * jnp.dot(
+        expand.astype(F32), gates, precision=lax.Precision.HIGHEST, preferred_element_type=F32
+    )
+    gate_cols = jnp.transpose(gate_rows)
+    gate_hi = gate_cols.astype(BF16)
+    gate_lo = (gate_cols - gate_hi.astype(F32)).astype(BF16)
+
     mark("r6_wait")
     arrived(8, rr, N - 1)
 
@@ -300,44 +339,44 @@
     mix = (dot(gate_hi, back) + dot(gate_lo, back)).astype(BF16)
     for j in range(N // 2):
         sm[j] = mix[:, j * PIECE : (j + 1) * PIECE]
-    for step in range(1, N // 2):
-        to = around(z, step, N // 2)
+    for d in FAR:
+        to = lax.rem(z + d, N // 2)
         send(9, sm.at[to], rm.at[z], tp=2 * to + c)
     sent(9, sm, N // 2 - 1)
     rm[z] = sm[z]
     mark("r7_wait")
     arrived(9, rm, N // 2 - 1)
     mark("stats_s8")
-    own = nrm[:, pl.ds(pl.multiple_of(t * PIECE, PIECE), PIECE)].astype(F32)
+    own = nrm[:, pl.ds(pl.multiple_of(z * PIECE, PIECE), PIECE)].astype(F32)
     u = ALPHA * own + jnp.sum(rm[...].astype(F32), axis=0)
 
-    part_mean = jnp.mean(u, axis=1, keepdims=True)
-    part_sq = jnp.sum((u - part_mean) ** 2, axis=1, keepdims=True)
-    lane, row = iota((ROWS, LANES), 1), iota((ROWS, LANES), 0)
-    line = jnp.where(lane == row, part_mean, jnp.where(lane == row + ROWS, part_sq, 0.0))
-    ss[...] = jnp.sum(line, axis=0, keepdims=True)
-    for step in range(1, N):
-        to = around(t, step, N)
-        send(10, ss, rs.at[t], tp=to)
-    sent(10, rs, N - 1)
-    rs[t] = ss[...]
+    ss[1] = moments(u)
+    for p in ALL_TP:
+        send(10, ss.at[1], rs.at[1, t], tp=tp_at(*p))
+    sent(10, rs.at[1], N - 1)
+    rs[1, t] = ss[1]
     mark("r8_wait")
     fetched(15)
-    arrived(10, rs, N - 1)
+    arrived(10, rs.at[1], N - 1)
     mark("final")
-    means = jnp.concatenate([rs[i] for i in range(N)], axis=0)
-    total = jnp.sum(means, axis=0, keepdims=True)
-    spread_sq = jnp.sum((means - total / N) ** 2, axis=0, keepdims=True)
-    mean = jnp.sum(jnp.where(lane == row, total / N, 0.0), axis=1, keepdims=True)
-    between = jnp.sum(jnp.where(lane == row, spread_sq, 0.0), axis=1, keepdims=True)
-    within = jnp.sum(jnp.where(lane == row + ROWS, total, 0.0), axis=1, keepdims=True)
-    variance = (within + PIECE * between) / D
-    out_ref[...] = ((u - mean) * lax.rsqrt(variance + EPSILON) * fg[...]).astype(BF16)
+    mean, scale = merged(rs[1])
+    out_ref[...] = ((u - mean) * scale * fg[...]).astype(BF16)
 
     mark("drain")
     for phase, like, count in pending:
         whole(phase, like, count).wait_send()
     mark(None)
+
+
+def written_out(out, state, out_h, state_h, sems):
+    copies = [
+        pltpu.make_async_copy(state, state_h, sems.at[0]),
+        pltpu.make_async_copy(out, out_h, sems.at[1]),
+    ]
+    for copy in copies:
+        copy.start()
+    for copy in copies:
+        copy.wait()
 
 
 def step(
@@ -346,7 +385,7 @@
 ):
     hbm = pl.BlockSpec(memory_space=pl.ANY)
     vmem, dma = pltpu.VMEM, pltpu.SemaphoreType.DMA
-    return pl.pallas_call(
+    results = pl.pallas_call(
         kernel,
         out_shape=(
             pltpu.VMEM((ROWS, PIECE), BF16),
@@ -359,14 +398,14 @@
             vmem((N, D), BF16), vmem((16, KEYS), F32), vmem((1, KEYS), F32), vmem((ROWS, KEYS, LANES), F32),
             vmem((LANES, D), BF16), vmem((1, D), F32), vmem((N, D), BF16), vmem((2, ROWS), jnp.int32),
             vmem((D, 2 * LANES), BF16), vmem((LANES, D), BF16), vmem((1, PIECE), F32),
-            vmem((N, ROWS, LANES), BF16), vmem((N, ROWS, LANES), BF16), vmem((4, ROWS, LANES), BF16),
+            vmem((2, 4, ROWS, KEYS), BF16), vmem((N, ROWS, KEYS), BF16), vmem((2, ROWS, KEYS), BF16),
             vmem((ROWS, LANES), F32), vmem((N, ROWS, PIECE), BF16), vmem((N, ROWS, PIECE), BF16),
-            vmem((N, ROWS, PIECE), BF16), vmem((ROWS, D), F32), vmem((ROWS, D), BF16),
+            vmem((N // 2, ROWS, PIECE), BF16), vmem((ROWS, HALF), BF16),
             vmem((N, CAP, HALF), BF16), vmem((N, CAP, HALF), BF16), vmem((N, CAP, HALF), BF16),
             vmem((N * CAP, HALF), F32), vmem((N // 2, N * CAP, PIECE), BF16), vmem((N // 2, N * CAP, PIECE), BF16),
             vmem((N, CAP, HALF), BF16), vmem((N, CAP, HALF), BF16), vmem((N // 2, ROWS, PIECE), BF16),
-            vmem((N // 2, ROWS, PIECE), BF16), vmem((1, LANES), F32), vmem((N, 1, LANES), F32),
-            dma((16,)), dma((11,)), dma((11,)),
+            vmem((N // 2, ROWS, PIECE), BF16), vmem((2, 1, LANES), F32), vmem((2, N, 1, LANES), F32), vmem((2, N, LANES), F32),
+            dma((16,)), dma((13,)), dma((13,)),
         ],
         compiler_params=pltpu.CompilerParams(
             collective_id=0, has_side_effects=True, vmem_limit_bytes=60 * 1024 * 1024
@@ -377,6 +416,15 @@
         out_weight, norm_gain.reshape(1, -1), router_weight.T, routing.T, glu_weight, linear_weight, down_weight,
         final_gain.reshape(1, -1),
     )
+    results = [pltpu.with_memory_space_constraint(r, pltpu.VMEM) for r in results]
+    return pl.pallas_call(
+        written_out,
+        out_shape=tuple(jax.ShapeDtypeStruct(r.shape, r.dtype) for r in results),
+        in_specs=[pl.BlockSpec(memory_space=pltpu.VMEM)] * 2,
+        out_specs=(hbm, hbm),
+        scratch_shapes=[dma((2,))],
+        name="written_out",
+    )(*results)
 
 
 def solution(mesh):

time: 60.8 us -> 55.9 us (0.919)
  Pallas kernels: 58.2 us -> 55.2 us
  local copies, waits for them, and re-layouts: 1.92 us -> 0 us
    pallas_call x1, Pallas kernels: 58.2 us -> 53.8 us  [step(): pl.pallas_call(kernel, out_shape=(pltpu.VMEM((ROWS, PIECE), BF16), pltpu....]
    unnamed x2 -> x0, local copies, waits for them, and re-layouts: 1.92 us -> none
    pallas_call x0 -> x1, Pallas kernels: none -> 1.34 us  [step(): pl.pallas_call(written_out, out_shape=tuple((jax.ShapeDtypeStruct(r.shape...]
where the time goes in v3:
time: 55.9 us; the launch traced here: 55.8 us
  Pallas kernels  55.2 us (99%)
  between operations  0.64 us (1%)
    pallas_call x1, Pallas kernels, step(): pl.pallas_call(kernel, out_shape=(pltpu.VMEM((ROWS, PIECE), BF16), pltpu....  53.8 us
    pallas_call x1, Pallas kernels, step(): pl.pallas_call(written_out, out_shape=tuple((jax.ShapeDtypeStruct(r.shape...  1.34 us

profile of v3, /device:TPU:1, one launch (start us, length us, event | category | flops | bytes accessed | tf_op | source)
XLA Modules:
  0.0 55.8 jit_solution(1958197833631787590)
XLA Ops:
  0.6 53.8 %decode_step.1 = (bf16[16,256]{1,0:T(8,128)(2,1)S(1)}, f32[16,256,128]{2,1,0:T(8,128)S(1)}) custom-call(bf16[16,4096]{1,0:T(8,128)(2,1)} %tok_h.1, bf16[256,1024]{1,0:T(8,128)(2,1)} %qw_h.1, bf16[256,1024]{1,0:T(8,128)(2,1)} %kw_h.1, bf16[4096,128]{1,0:T(8,128)(2,1)} %vw_h.1, bf16[16,4096]{1,0:T(8,128)(2,1)} %bitcast.6, f32[16,1024]{1,0:T(8,128)} %du_h.1, ...), custom_call_target="tpu_custom_call" | custom-call | tf_op jit(solution)/shard_map/decode_step/pallas_call | solution.py:388
  54.5 1.3 %written_out.1 = (bf16[16,256]{1,0:T(8,128)(2,1)}, f32[16,256,128]{2,1,0:T(8,128)}) custom-call(bf16[16,256]{1,0:T(8,128)(2,1)S(1)} %get-tuple-element.4.out, f32[16,256,128]{2,1,0:T(8,128)S(1)} %get-tuple-element.5.state), custom_call_target="tpu_custom_call" | custom-call | tf_op jit(solution)/shard_map/written_out/pallas_call | solution.py:420

commit v4 on v3

--- a/solution.py
+++ b/solution.py
@@ -87,8 +87,8 @@
 def kernel(
     tok_h, qw_h, kw_h, vw_h, dd_h, du_h, db_h, st_h, ow_h, ng_h, rw_h, rt_h, glu_h, lin_h, dn_h, fg_h,
     out_ref, ns,
-    tok, qw, kw, vw, dd, du, db, st, ow, ng, rw, rt, gl, dn, fg,
-    sq, rq, rqk, mixed, sp, rp, rg, nrm, sd, rd, rd2, xs, sh, rh, sr, rr, sm, rm, ss, rs, lg,
+    tok, qw, kw, vw, dd, du, db, st, ow, ng, rw, rt, gl, dn, fg, decayed,
+    sq, rq, rqk, mixed, sp, rp, rg, nrm, sd, rd, su, ru, sr, rr, sm, rm, ss, rs, lg,
     loc, out_sem, in_sem,
 ):
     e = lax.axis_index("ep")
@@ -109,12 +109,23 @@
     fetches = [
         (tok_h, tok), (qw_h, qw), (kw_h, kw), (dd_h, dd), (du_h.at[:, head_cols], du), (db_h.at[:, head_cols], db),
         (vw_h, vw), (st_h, st), (ow_h, ow), (ng_h, ng), (rw_h, rw), (rt_h, rt),
-        (glu_h.at[0], gl.at[:, pl.ds(0, LANES)]), (lin_h.at[0], gl.at[:, pl.ds(LANES, LANES)]),
-        (dn_h.at[0], dn), (fg_h.at[:, pl.ds(pl.multiple_of(t * PIECE, PIECE), PIECE)], fg),
+        (fg_h.at[:, pl.ds(pl.multiple_of(t * PIECE, PIECE), PIECE)], fg),
     ]
     copies = [pltpu.make_async_copy(a, b, loc.at[i]) for i, (a, b) in enumerate(fetches)]
     for copy in copies:
         copy.start()
+
+    units = pl.ds(pl.multiple_of(c * LANES, LANES), LANES)
+    linear_units = pl.ds(pl.multiple_of((2 + c) * LANES, LANES), LANES)
+
+    def expert_weights(core):
+        blocks = [(glu_h.at[:, core], gl.at[:, :, units]), (lin_h.at[:, core], gl.at[:, :, linear_units])]
+        for j in range(N // 2):
+            cols = pl.ds(pl.multiple_of((2 * j + core) * PIECE, PIECE), PIECE)
+            blocks.append((dn_h.at[0, :, cols], dn.at[j, units, :]))
+        return blocks
+
+    own_weights = [pltpu.make_async_copy(a, b, loc.at[13 + i]) for i, (a, b) in enumerate(expert_weights(c))]
 
     def fetched(*which):
         for i in which:
@@ -159,6 +170,10 @@
         to = tp_at(d, x)
         send(0, sq.at[lax.rem(to, 2), to // 4], rq.at[t], tp=to)
     sent(0, rq, N - 1)
+    for copy in own_weights:
+        copy.start()
+    for i, (mine, theirs) in enumerate(expert_weights(1 - c)):
+        send(min(13 + i, 15), mine, theirs, tp=partner)
     rq[t] = sq[c, head]
 
     mark("decay")
@@ -180,7 +195,7 @@
     mark("state_decay")
     fetched(7)
     for s in range(ROWS):
-        ns[s] = decay_wide[:, s * LANES : (s + 1) * LANES] * st[s]
+        decayed[s] = decay_wide[:, s * LANES : (s + 1) * LANES] * st[s]
     own_block = iota((ROWS, wide), 0) == iota((ROWS, wide), 1) // LANES
     ones1 = own_block.astype(BF16)
     values_f = values.astype(F32)
@@ -195,17 +210,15 @@
     arrived(1, rqk, 1)
     mark("state")
     query, keys = rqk[0].astype(F32), rqk[1].astype(F32)
-    update = dot(jnp.transpose(keys).astype(BF16), values_wide)
     query_wide = dot(jnp.transpose(query).astype(BF16), ones1)
     for s in range(ROWS):
         cols = slice(s * LANES, (s + 1) * LANES)
-        new = ns[s] + update[:, cols]
-        ns[s] = new
-        mixed[s : s + 1, :] = jnp.sum(query_wide[:, cols] * new, axis=0, keepdims=True)
-
+        mixed[s : s + 1, :] = jnp.sum(query_wide[:, cols] * decayed[s], axis=0, keepdims=True)
+    match = jnp.sum(query * keys, axis=1, keepdims=True)
     mark("out_dot_s2")
     fetched(8)
-    attn_part = dot((mixed[...] * KEYS ** (-0.5)).astype(BF16), ow[...]).astype(BF16)
+    readout = (mixed[...] + match * values_f) * KEYS ** (-0.5)
+    attn_part = dot(readout.astype(BF16), ow[...]).astype(BF16)
     for i in range(N):
         sp[i] = attn_part[:, i * PIECE : (i + 1) * PIECE]
     for p in ALL_TP:
@@ -214,6 +227,10 @@
     sent(2, sp, N - 1)
     rp[t] = sp[t]
 
+    mark("update")
+    update = dot(jnp.transpose(keys).astype(BF16), values_wide)
+    for s in range(ROWS):
+        ns[s] = decayed[s] + update[:, s * LANES : (s + 1) * LANES]
     mark("slots")
     fetched(9, 10, 11)
     slots = N * CAP
@@ -254,15 +271,11 @@
         nrm[:, j * PIECE : (j + 1) * PIECE] = ((hidden - mean) * scale * ng[:, block(j, c)]).astype(BF16)
 
     mark("s4_send")
-    packed = dot(spread.astype(BF16), nrm[...])
-    for i in range(N):
-        sd[i] = packed[i * CAP : (i + 1) * CAP].astype(BF16)
+    sd[...] = dot(spread.astype(BF16), nrm[...]).astype(BF16).reshape(N, CAP, HALF)
     for p in ALL_EP:
         to = ep_at(*p)
         send(4, sd.at[to], rd.at[e], ep=to)
     sent(4, sd, N - 1)
-    send(5, sd.at[e], rd2.at[e], tp=partner)
-    sent(5, sd, 1)
     rd[e] = sd[e]
 
     mark("gates")
@@ -274,43 +287,29 @@
 
     mark("r4_wait_fwd")
     arrived(4, rd, N - 1)
-    for p in ALL_EP:
-        src = ep_at(*p)
-        send(6, rd.at[src], rd2.at[src], tp=partner)
-    sent(6, rd, N - 1)
-    mark("up_own")
-    fetched(12, 13)
-    for i in range(N):
-        xs[i * CAP : (i + 1) * CAP, :] = rd[i].astype(F32)
-    rows = xs[...].astype(BF16)
-    pre_act = sum(dot(rows[:, j * PIECE : (j + 1) * PIECE], gl[block(j, c), :]) for j in range(N // 2))
-    mark("r4d_wait")
-    arrived(5, rd2, 1)
-    arrived(6, rd2, N - 1)
-    mark("up_other")
-    for i in range(N):
-        xs[i * CAP : (i + 1) * CAP, :] = rd2[i].astype(F32)
-    rows = xs[...].astype(BF16)
-    pre_act += sum(dot(rows[:, j * PIECE : (j + 1) * PIECE], gl[block(j, 1 - c), :]) for j in range(N // 2))
-    glu = jnp.minimum(pre_act[:, :LANES], LIMIT)
-    linear = jnp.clip(pre_act[:, LANES:], -LIMIT, LIMIT)
+    mark("up")
+    rows = rd[...].reshape(N * CAP, HALF)
+    for copy in own_weights[:2]:
+        copy.wait()
+    arrived(13, gl.at[:, :, pl.ds(0, LANES)], None)
+    arrived(14, gl.at[:, :, pl.ds(0, LANES)], None)
+    su[...] = dot(rows, gl[...].reshape(HALF, 4 * LANES))
+    send(5, su, ru, tp=partner)
+    sent(5, su, None)
+    mark("up_wait")
+    arrived(5, ru, None)
+    mark("down")
+    pre_act = su[...] + ru[...]
+    glu = jnp.minimum(pre_act[:, : 2 * LANES], LIMIT)
+    linear = jnp.clip(pre_act[:, 2 * LANES :], -LIMIT, LIMIT)
     act = (glu * jax.nn.sigmoid(SLOPE * glu) * (linear + 1.0)).astype(BF16)
 
     mark("down")
-    fetched(14)
-    theirs = [dot(act, dn[:, block(j, 1 - c)]) for j in range(N // 2)]
+    for copy in own_weights[2:]:
+        copy.wait()
+    arrived(15, dn.at[:, pl.ds(0, LANES), :], None)
     for j in range(N // 2):
-        sh[j] = theirs[j].astype(BF16)
-    send(7, sh, rh, tp=partner)
-    sent(7, sh, None)
-    mine = [dot(act, dn[:, block(j, c)]) for j in range(N // 2)]
-    mark("down_wait")
-    arrived(7, rh, None)
-    mark("down_sum")
-    for j in range(N // 2):
-        total = (mine[j] + rh[j].astype(F32)).astype(BF16)
-        for i in range(N):
-            sr[i, :, j * PIECE : (j + 1) * PIECE] = total[i * CAP : (i + 1) * CAP]
+        sr[:, :, j * PIECE : (j + 1) * PIECE] = dot(act, dn[j]).astype(BF16).reshape(N, CAP, PIECE)
     mark("s6_send")
     for p in ALL_EP:
         to = ep_at(*p)
@@ -333,9 +332,7 @@
     arrived(8, rr, N - 1)
 
     mark("mix_s7")
-    for i in range(N):
-        xs[i * CAP : (i + 1) * CAP, :] = rr[i].astype(F32)
-    back = xs[...].astype(BF16)
+    back = rr[...].reshape(N * CAP, HALF)
     mix = (dot(gate_hi, back) + dot(gate_lo, back)).astype(BF16)
     for j in range(N // 2):
         sm[j] = mix[:, j * PIECE : (j + 1) * PIECE]
@@ -356,23 +353,25 @@
     sent(10, rs.at[1], N - 1)
     rs[1, t] = ss[1]
     mark("r8_wait")
-    fetched(15)
+    fetched(12)
     arrived(10, rs.at[1], N - 1)
     mark("final")
     mean, scale = merged(rs[1])
     out_ref[...] = ((u - mean) * scale * fg[...]).astype(BF16)
 
     mark("drain")
+    sent(13, gl.at[:, :, pl.ds(0, LANES)], None)
+    sent(14, gl.at[:, :, pl.ds(0, LANES)], None)
+    sent(15, dn.at[:, pl.ds(0, LANES), :], None)
     for phase, like, count in pending:
         whole(phase, like, count).wait_send()
     mark(None)
 
 
 def written_out(out, state, out_h, state_h, sems):
-    copies = [
-        pltpu.make_async_copy(state, state_h, sems.at[0]),
-        pltpu.make_async_copy(out, out_h, sems.at[1]),
-    ]
+    rows = [pl.ds(2 * i, 2) for i in range(ROWS // 2)]
+    copies = [pltpu.make_async_copy(state.at[r], state_h.at[r], sems.at[i]) for i, r in enumerate(rows)]
+    copies.append(pltpu.make_async_copy(out, out_h, sems.at[ROWS // 2]))
     for copy in copies:
         copy.start()
     for copy in copies:
@@ -384,6 +383,10 @@
     norm_gain, router_weight, routing, glu_weight, linear_weight, down_weight, final_gain,
 ):
     hbm = pl.BlockSpec(memory_space=pl.ANY)
+
+    def in_blocks(weight):
+        return weight.reshape(N // 2, 2, PIECE, LANES)
+
     vmem, dma = pltpu.VMEM, pltpu.SemaphoreType.DMA
     results = pl.pallas_call(
         kernel,
@@ -397,15 +400,15 @@
             vmem((ROWS, D), BF16), vmem((PIECE, 1024), BF16), vmem((PIECE, 1024), BF16), vmem((D, LANES), BF16),
             vmem((N, D), BF16), vmem((16, KEYS), F32), vmem((1, KEYS), F32), vmem((ROWS, KEYS, LANES), F32),
             vmem((LANES, D), BF16), vmem((1, D), F32), vmem((N, D), BF16), vmem((2, ROWS), jnp.int32),
-            vmem((D, 2 * LANES), BF16), vmem((LANES, D), BF16), vmem((1, PIECE), F32),
+            vmem((N // 2, PIECE, 4 * LANES), BF16), vmem((N // 2, 2 * LANES, PIECE), BF16), vmem((1, PIECE), F32), vmem((ROWS, KEYS, LANES), F32),
             vmem((2, 4, ROWS, KEYS), BF16), vmem((N, ROWS, KEYS), BF16), vmem((2, ROWS, KEYS), BF16),
             vmem((ROWS, LANES), F32), vmem((N, ROWS, PIECE), BF16), vmem((N, ROWS, PIECE), BF16),
             vmem((N // 2, ROWS, PIECE), BF16), vmem((ROWS, HALF), BF16),
-            vmem((N, CAP, HALF), BF16), vmem((N, CAP, HALF), BF16), vmem((N, CAP, HALF), BF16),
-            vmem((N * CAP, HALF), F32), vmem((N // 2, N * CAP, PIECE), BF16), vmem((N // 2, N * CAP, PIECE), BF16),
+            vmem((N, CAP, HALF), BF16), vmem((N, CAP, HALF), BF16),
+            vmem((N * CAP, 4 * LANES), F32), vmem((N * CAP, 4 * LANES), F32),
             vmem((N, CAP, HALF), BF16), vmem((N, CAP, HALF), BF16), vmem((N // 2, ROWS, PIECE), BF16),
             vmem((N // 2, ROWS, PIECE), BF16), vmem((2, 1, LANES), F32), vmem((2, N, 1, LANES), F32), vmem((2, N, LANES), F32),
-            dma((16,)), dma((13,)), dma((13,)),
+            dma((24,)), dma((16,)), dma((16,)),
         ],
         compiler_params=pltpu.CompilerParams(
             collective_id=0, has_side_effects=True, vmem_limit_bytes=60 * 1024 * 1024
@@ -413,7 +416,7 @@
         name="decode_step",
     )(
         tokens, query_weight, key_weight, value_weight, decay_down.T, decay_up, decay_bias.reshape(1, -1), old_state,
-        out_weight, norm_gain.reshape(1, -1), router_weight.T, routing.T, glu_weight, linear_weight, down_weight,
+        out_weight, norm_gain.reshape(1, -1), router_weight.T, routing.T, in_blocks(glu_weight), in_blocks(linear_weight), down_weight,
         final_gain.reshape(1, -1),
     )
     results = [pltpu.with_memory_space_constraint(r, pltpu.VMEM) for r in results]
@@ -422,7 +425,7 @@
         out_shape=tuple(jax.ShapeDtypeStruct(r.shape, r.dtype) for r in results),
         in_specs=[pl.BlockSpec(memory_space=pltpu.VMEM)] * 2,
         out_specs=(hbm, hbm),
-        scratch_shapes=[dma((2,))],
+        scratch_shapes=[dma((ROWS // 2 + 1,))],
         name="written_out",
     )(*results)
 

time: 55.9 us -> 54 us (0.966)
  Pallas kernels: 55.2 us -> 53.3 us
    pallas_call x1, Pallas kernels: 53.8 us -> 51.9 us  [step(): pl.pallas_call(kernel, out_shape=(pltpu.VMEM((ROWS, PIECE), BF16), pltpu....]
where the time goes in v4:
time: 54 us
  Pallas kernels  53.3 us (99%)
  between operations  0.64 us (1%)
    pallas_call x1, Pallas kernels, step(): pl.pallas_call(kernel, out_shape=(pltpu.VMEM((ROWS, PIECE), BF16), pltpu....  51.9 us
    pallas_call x1, Pallas kernels, step(): pl.pallas_call(written_out, out_shape=tuple((jax.ShapeDtypeStruct(r.shape...  1.39 us

profile of v4, /device:TPU:1, one launch (start us, length us, event | category | flops | bytes accessed | tf_op | source)
XLA Modules:
  0.0 54.0 jit_solution(15804066620970700642)
XLA Ops:
  0.6 51.9 %decode_step.1 = (bf16[16,256]{1,0:T(8,128)(2,1)S(1)}, f32[16,256,128]{2,1,0:T(8,128)S(1)}) custom-call(bf16[16,4096]{1,0:T(8,128)(2,1)} %tok_h.1, bf16[256,1024]{1,0:T(8,128)(2,1)} %qw_h.1, bf16[256,1024]{1,0:T(8,128)(2,1)} %kw_h.1, bf16[4096,128]{1,0:T(8,128)(2,1)} %vw_h.1, bf16[16,4096]{1,0:T(8,128)(2,1)} %bitcast.10, f32[16,1024]{1,0:T(8,128)} %du_h.1, ...), custom_call_target="tpu_custom_call" | custom-call | tf_op jit(solution)/shard_map/decode_step/pallas_call | solution.py:391
  52.6 1.4 %written_out.1 = (bf16[16,256]{1,0:T(8,128)(2,1)}, f32[16,256,128]{2,1,0:T(8,128)}) custom-call(bf16[16,256]{1,0:T(8,128)(2,1)S(1)} %get-tuple-element.4.out, f32[16,256,128]{2,1,0:T(8,128)S(1)} %get-tuple-element.5.state), custom_call_target="tpu_custom_call" | custom-call | tf_op jit(solution)/shard_map/written_out/pallas_call | solution.py:423

commit v5 on v4

--- a/solution.py
+++ b/solution.py
@@ -22,6 +22,7 @@
 PIECE = 256
 HALF = 2048
 CAP = 4
+PART = 8
 KEYS = 256
 LANES = 128
 FAR = (4, 3, 5, 2, 6, 1, 7)
@@ -87,8 +88,8 @@
 def kernel(
     tok_h, qw_h, kw_h, vw_h, dd_h, du_h, db_h, st_h, ow_h, ng_h, rw_h, rt_h, glu_h, lin_h, dn_h, fg_h,
     out_ref, ns,
-    tok, qw, kw, vw, dd, du, db, st, ow, ng, rw, rt, gl, dn, fg, decayed,
-    sq, rq, rqk, mixed, sp, rp, rg, nrm, sd, rd, su, ru, sr, rr, sm, rm, ss, rs, lg,
+    tok, qw, kw, vw, dd, du, db, st, ow, ng, rw, rt, gl, dn, fg, tok_part, decayed,
+    sq, rq, vals, val_out, mixed, sp, rp, rg, hid, nrm, sd, rd, su, ru, sr, rr, sm, rm, ss, rs, ns_in,
     loc, out_sem, in_sem,
 ):
     e = lax.axis_index("ep")
@@ -105,18 +106,23 @@
         return 4 * lax.rem(e // 4 + dy, 4) + lax.rem(lax.rem(e, 4) + dx, 4)
 
     mark("fetch")
+    units = pl.ds(pl.multiple_of(c * LANES, LANES), LANES)
+    linear_units = pl.ds(pl.multiple_of((2 + c) * LANES, LANES), LANES)
+
+    def rows_of(core):
+        return pl.ds(pl.multiple_of(core * PART, PART), PART)
+
     head_cols = pl.ds(pl.multiple_of(head * KEYS, KEYS), KEYS)
     fetches = [
         (tok_h, tok), (qw_h, qw), (kw_h, kw), (dd_h, dd), (du_h.at[:, head_cols], du), (db_h.at[:, head_cols], db),
-        (vw_h, vw), (st_h, st), (ow_h, ow), (ng_h, ng), (rw_h, rw), (rt_h, rt),
+        (vw_h, vw), (st_h.at[rows_of(c)], st.at[c]), (ow_h, ow.at[units, :]), (ng_h, ng), (rw_h, rw), (rt_h, rt),
         (fg_h.at[:, pl.ds(pl.multiple_of(t * PIECE, PIECE), PIECE)], fg),
+        (tok_h.at[rows_of(c), :], tok_part),
     ]
     copies = [pltpu.make_async_copy(a, b, loc.at[i]) for i, (a, b) in enumerate(fetches)]
     for copy in copies:
         copy.start()
 
-    units = pl.ds(pl.multiple_of(c * LANES, LANES), LANES)
-    linear_units = pl.ds(pl.multiple_of((2 + c) * LANES, LANES), LANES)
 
     def expert_weights(core):
         blocks = [(glu_h.at[:, core], gl.at[:, :, units]), (lin_h.at[:, core], gl.at[:, :, linear_units])]
@@ -125,7 +131,7 @@
             blocks.append((dn_h.at[0, :, cols], dn.at[j, units, :]))
         return blocks
 
-    own_weights = [pltpu.make_async_copy(a, b, loc.at[13 + i]) for i, (a, b) in enumerate(expert_weights(c))]
+    own_weights = [pltpu.make_async_copy(a, b, loc.at[14 + i]) for i, (a, b) in enumerate(expert_weights(c))]
 
     def fetched(*which):
         for i in which:
@@ -146,8 +152,9 @@
     k_part = dot(share, kw[...]).astype(BF16)
     for i in range(4):
         cols = slice(i * KEYS, (i + 1) * KEYS)
-        sq[0, i] = q_part[:, cols]
-        sq[1, i] = k_part[:, cols]
+        both = jnp.concatenate([q_part[:, cols], k_part[:, cols]], axis=1)
+        sq[0, i] = both[:PART]
+        sq[1, i] = both[PART:]
     mark("barrier_wait")
     pl.semaphore_wait(barrier, 2 * (N - 1))
     mark("s1_send")
@@ -170,17 +177,19 @@
         to = tp_at(d, x)
         send(0, sq.at[lax.rem(to, 2), to // 4], rq.at[t], tp=to)
     sent(0, rq, N - 1)
-    for copy in own_weights:
-        copy.start()
-    for i, (mine, theirs) in enumerate(expert_weights(1 - c)):
-        send(min(13 + i, 15), mine, theirs, tp=partner)
+    send(11, st_h.at[rows_of(1 - c)], st.at[c], tp=partner)
+    send(12, ow_h, ow.at[units, :], tp=partner)
     rq[t] = sq[c, head]
 
     mark("decay")
-    fetched(3, 4, 5, 6)
-    tokens = tok[...]
-    values = dot(tokens, vw[...]).astype(BF16)
-    low_rank = dot_nt(tokens, dd[...])
+    fetched(3, 4, 5, 6, 13)
+    values = dot(tok[...], vw[...]).astype(BF16).astype(F32)
+    mine_first = c == 0
+    val_out[...] = jnp.where(mine_first, values[PART:], values[:PART])
+    vals[c] = jnp.where(mine_first, values[:PART], values[PART:])
+    send(1, val_out, vals.at[c], tp=partner)
+    sent(1, val_out, None)
+    low_rank = dot_nt(tok_part[...], dd[...])
     pre = jnp.dot(low_rank, du[...], precision=lax.Precision.HIGHEST, preferred_element_type=F32) + db[...]
     log_sig = -(jnp.maximum(-pre, 0.0) + jnp.log1p(jnp.exp(-jnp.abs(pre))))
     decay = jnp.exp(log_sig / TAU)
@@ -189,48 +198,56 @@
     mid = rest.astype(BF16)
     low = (rest - mid.astype(F32)).astype(BF16)
     thirds = jnp.concatenate([hi.astype(F32), mid.astype(F32), low.astype(F32)], axis=0)
-    wide = ROWS * LANES
-    ones3 = (lax.rem(iota((3 * ROWS, wide), 0), ROWS) == iota((3 * ROWS, wide), 1) // LANES).astype(BF16)
+    wide = PART * LANES
+    ones3 = (lax.rem(iota((3 * PART, wide), 0), PART) == iota((3 * PART, wide), 1) // LANES).astype(BF16)
     decay_wide = dot(jnp.transpose(thirds).astype(BF16), ones3)
     mark("state_decay")
     fetched(7)
-    for s in range(ROWS):
-        decayed[s] = decay_wide[:, s * LANES : (s + 1) * LANES] * st[s]
-    own_block = iota((ROWS, wide), 0) == iota((ROWS, wide), 1) // LANES
+    arrived(11, st.at[0], None)
+    for g in range(2):
+        for s in range(PART):
+            decayed[g, s] = decay_wide[:, s * LANES : (s + 1) * LANES] * st[g, s]
+    own_block = iota((PART, wide), 0) == iota((PART, wide), 1) // LANES
     ones1 = own_block.astype(BF16)
-    values_f = values.astype(F32)
-    values_wide = jnp.where(own_block, jnp.concatenate([values_f] * ROWS, axis=1), 0.0).astype(BF16)
-
+    arrived(1, val_out, None)
+    values_f = jnp.concatenate([vals[0], vals[1]], axis=1)
+    values_wide = jnp.concatenate(
+        [jnp.where(own_block, jnp.concatenate([vals[g]] * PART, axis=1), 0.0).astype(BF16) for g in range(2)], axis=1
+    )
     mark("r1_wait")
     arrived(0, rq, N - 1)
-    mark("r1_sum_r1b")
-    rqk[c] = jnp.sum(rq[...].astype(F32), axis=0).astype(BF16)
-    send(1, rqk.at[c], rqk.at[c], tp=partner)
-    sent(1, rqk, 1)
-    arrived(1, rqk, 1)
     mark("state")
-    query, keys = rqk[0].astype(F32), rqk[1].astype(F32)
+    query_keys = jnp.sum(rq[...].astype(F32), axis=0).astype(BF16).astype(F32)
+    query, keys = query_keys[:, :KEYS], query_keys[:, KEYS:]
     query_wide = dot(jnp.transpose(query).astype(BF16), ones1)
-    for s in range(ROWS):
-        cols = slice(s * LANES, (s + 1) * LANES)
-        mixed[s : s + 1, :] = jnp.sum(query_wide[:, cols] * decayed[s], axis=0, keepdims=True)
+    for g in range(2):
+        for s in range(PART):
+            spread_query = query_wide[:, s * LANES : (s + 1) * LANES]
+            line = jnp.sum(spread_query * decayed[g, s], axis=0, keepdims=True)
+            mixed[s : s + 1, g * LANES : (g + 1) * LANES] = line
     match = jnp.sum(query * keys, axis=1, keepdims=True)
     mark("out_dot_s2")
     fetched(8)
+    arrived(12, ow.at[pl.ds(0, LANES), :], None)
     readout = (mixed[...] + match * values_f) * KEYS ** (-0.5)
     attn_part = dot(readout.astype(BF16), ow[...]).astype(BF16)
-    for i in range(N):
-        sp[i] = attn_part[:, i * PIECE : (i + 1) * PIECE]
-    for p in ALL_TP:
-        to = tp_at(*p)
-        send(2, sp.at[to], rp.at[t], tp=to)
-    sent(2, sp, N - 1)
-    rp[t] = sp[t]
+    for i in range(N // 2):
+        sp[i] = attn_part[:, i * 2 * PIECE : (i + 1) * 2 * PIECE]
+    for d in FAR:
+        send(2, sp.at[lax.rem(z + d, N // 2)], rp.at[z], tp=tp_at(d, 0))
+    sent(2, rp, N // 2 - 1)
+    rp[z] = sp[z]
+    for copy in own_weights:
+        copy.start()
+    for i, (mine, theirs) in enumerate(expert_weights(1 - c)):
+        send(min(13 + i, 15), mine, theirs, tp=partner)
 
     mark("update")
     update = dot(jnp.transpose(keys).astype(BF16), values_wide)
-    for s in range(ROWS):
-        ns[s] = decayed[s] + update[:, s * LANES : (s + 1) * LANES]
+    for g in range(2):
+        for s in range(PART):
+            at = (g * PART + s) * LANES
+            decayed[g, s] = decayed[g, s] + update[:, at : at + LANES]
     mark("slots")
     fetched(9, 10, 11)
     slots = N * CAP
@@ -245,33 +262,35 @@
     spread = (here & (place == lax.rem(iota((slots, ROWS), 0), CAP).astype(F32))).astype(F32)
 
     mark("r2_wait")
-    arrived(2, rp, N - 1)
+    arrived(2, rp, N // 2 - 1)
     mark("s3_send")
-    rg[z] = jnp.sum(rp[...].astype(F32), axis=0).astype(BF16)
-    own_cols = pl.ds(pl.multiple_of(t * PIECE, PIECE), PIECE)
-    ss[0] = moments(ALPHA * tok[:, own_cols].astype(F32) + rg[z].astype(F32))
-    for d in FAR:
-        send(3, rg.at[z], rg.at[z], tp=tp_at(d, 0))
+    rg[t] = jnp.sum(rp[...].astype(F32), axis=0).astype(BF16)
     for p in ALL_TP:
-        send(11, ss.at[0], rs.at[0, t], tp=tp_at(*p))
-    rs[0, t] = ss[0]
-    sent(3, rg, N // 2 - 1)
-    sent(11, rs.at[0], N - 1)
+        send(3, rg.at[t], rg.at[t], tp=tp_at(*p))
+    sent(3, rg, N - 1)
+    send(10, decayed.at[1 - c], ns_in, tp=partner)
+    sent(10, ns_in, None)
+    for s in range(PART):
+        ns[c * PART + s] = decayed[c, s]
     mark("r3_wait")
-    arrived(11, rs.at[0], N - 1)
-    mean, scale = merged(rs[0])
-    arrived(3, rg, N // 2 - 1)
+    arrived(3, rg, N - 1)
 
     mark("norm1")
     def block(j, core):
         return pl.ds(pl.multiple_of((2 * j + core) * PIECE, PIECE), PIECE)
 
-    for j in range(N // 2):
-        hidden = ALPHA * tok[:, block(j, c)].astype(F32) + rg[j].astype(F32)
-        nrm[:, j * PIECE : (j + 1) * PIECE] = ((hidden - mean) * scale * ng[:, block(j, c)]).astype(BF16)
+    for i in range(N // 2):
+        cols = slice(i * 2 * PIECE, (i + 1) * 2 * PIECE)
+        attn = jnp.concatenate([rg[2 * i].astype(F32), rg[2 * i + 1].astype(F32)], axis=0)
+        hid[:, cols] = ALPHA * tok[:, cols].astype(F32) + attn
+    hidden = hid[...]
+    centred = hidden - jnp.mean(hidden, axis=1, keepdims=True)
+    var = jnp.mean(centred * centred, axis=1, keepdims=True)
+    nrm[...] = (centred * lax.rsqrt(var + EPSILON) * ng[...]).astype(BF16)
 
     mark("s4_send")
-    sd[...] = dot(spread.astype(BF16), nrm[...]).astype(BF16).reshape(N, CAP, HALF)
+    half = jnp.concatenate([nrm[:, block(j, c)] for j in range(N // 2)], axis=1)
+    sd[...] = dot(spread.astype(BF16), half).astype(BF16).reshape(N, CAP, HALF)
     for p in ALL_EP:
         to = ep_at(*p)
         send(4, sd.at[to], rd.at[e], ep=to)
@@ -279,11 +298,10 @@
     rd[e] = sd[e]
 
     mark("gates")
-    rw_half = jnp.concatenate([rw[:, block(j, c)] for j in range(N // 2)], axis=1)
-    logit_part = dot_nt(rw_half, nrm[...])
-    lg[c] = jnp.concatenate([logit_part, jnp.zeros((N, LANES - ROWS), F32)], axis=1)
-    send(12, lg.at[c], lg.at[c], tp=partner)
-    sent(12, lg, 1)
+    logits = dot_nt(rw[...], nrm[...])
+    arrived(10, ns_in, None)
+    for s in range(PART):
+        ns[(1 - c) * PART + s] = ns_in[s]
 
     mark("r4_wait_fwd")
     arrived(4, rd, N - 1)
@@ -317,8 +335,6 @@
     sent(8, sr, N - 1)
     rr[e] = sr[e]
     mark("gates2")
-    arrived(12, lg, 1)
-    logits = (lg[0] + lg[1])[:, :ROWS]
     raised = jnp.where(chosen > 0.5, jnp.exp(logits), 0.0)
     gates = raised / jnp.sum(raised, axis=0, keepdims=True)
     gate_rows = spread * jnp.dot(
@@ -344,22 +360,24 @@
     mark("r7_wait")
     arrived(9, rm, N // 2 - 1)
     mark("stats_s8")
-    own = nrm[:, pl.ds(pl.multiple_of(z * PIECE, PIECE), PIECE)].astype(F32)
+    own = nrm[:, pl.ds(pl.multiple_of(t * PIECE, PIECE), PIECE)].astype(F32)
     u = ALPHA * own + jnp.sum(rm[...].astype(F32), axis=0)
 
-    ss[1] = moments(u)
+    ss[...] = moments(u)
     for p in ALL_TP:
-        send(10, ss.at[1], rs.at[1, t], tp=tp_at(*p))
-    sent(10, rs.at[1], N - 1)
-    rs[1, t] = ss[1]
+        send(6, ss, rs.at[t], tp=tp_at(*p))
+    sent(6, rs, N - 1)
+    rs[t] = ss[...]
     mark("r8_wait")
     fetched(12)
-    arrived(10, rs.at[1], N - 1)
+    arrived(6, rs, N - 1)
     mark("final")
-    mean, scale = merged(rs[1])
+    mean, scale = merged(rs)
     out_ref[...] = ((u - mean) * scale * fg[...]).astype(BF16)
 
     mark("drain")
+    sent(11, st.at[0], None)
+    sent(12, ow.at[pl.ds(0, LANES), :], None)
     sent(13, gl.at[:, :, pl.ds(0, LANES)], None)
     sent(14, gl.at[:, :, pl.ds(0, LANES)], None)
     sent(15, dn.at[:, pl.ds(0, LANES), :], None)
@@ -398,16 +416,16 @@
         out_specs=(pl.BlockSpec(memory_space=pltpu.VMEM), pl.BlockSpec(memory_space=pltpu.VMEM)),
         scratch_shapes=[
             vmem((ROWS, D), BF16), vmem((PIECE, 1024), BF16), vmem((PIECE, 1024), BF16), vmem((D, LANES), BF16),
-            vmem((N, D), BF16), vmem((16, KEYS), F32), vmem((1, KEYS), F32), vmem((ROWS, KEYS, LANES), F32),
-            vmem((LANES, D), BF16), vmem((1, D), F32), vmem((N, D), BF16), vmem((2, ROWS), jnp.int32),
-            vmem((N // 2, PIECE, 4 * LANES), BF16), vmem((N // 2, 2 * LANES, PIECE), BF16), vmem((1, PIECE), F32), vmem((ROWS, KEYS, LANES), F32),
-            vmem((2, 4, ROWS, KEYS), BF16), vmem((N, ROWS, KEYS), BF16), vmem((2, ROWS, KEYS), BF16),
-            vmem((ROWS, LANES), F32), vmem((N, ROWS, PIECE), BF16), vmem((N, ROWS, PIECE), BF16),
-            vmem((N // 2, ROWS, PIECE), BF16), vmem((ROWS, HALF), BF16),
+            vmem((N, D), BF16), vmem((16, KEYS), F32), vmem((1, KEYS), F32), vmem((2, PART, KEYS, LANES), F32),
+            vmem((2 * LANES, D), BF16), vmem((1, D), F32), vmem((N, D), BF16), vmem((2, ROWS), jnp.int32),
+            vmem((N // 2, PIECE, 4 * LANES), BF16), vmem((N // 2, 2 * LANES, PIECE), BF16), vmem((1, PIECE), F32), vmem((PART, D), BF16), vmem((2, PART, KEYS, LANES), F32),
+            vmem((2, 4, PART, 2 * KEYS), BF16), vmem((N, PART, 2 * KEYS), BF16), vmem((2, PART, LANES), F32),
+            vmem((PART, LANES), F32), vmem((PART, 2 * LANES), F32), vmem((N // 2, PART, 2 * PIECE), BF16),
+            vmem((N // 2, PART, 2 * PIECE), BF16), vmem((N, PART, 2 * PIECE), BF16), vmem((ROWS, D), F32), vmem((ROWS, D), BF16),
             vmem((N, CAP, HALF), BF16), vmem((N, CAP, HALF), BF16),
             vmem((N * CAP, 4 * LANES), F32), vmem((N * CAP, 4 * LANES), F32),
             vmem((N, CAP, HALF), BF16), vmem((N, CAP, HALF), BF16), vmem((N // 2, ROWS, PIECE), BF16),
-            vmem((N // 2, ROWS, PIECE), BF16), vmem((2, 1, LANES), F32), vmem((2, N, 1, LANES), F32), vmem((2, N, LANES), F32),
+            vmem((N // 2, ROWS, PIECE), BF16), vmem((1, LANES), F32), vmem((N, 1, LANES), F32), vmem((PART, KEYS, LANES), F32),
             dma((24,)), dma((16,)), dma((16,)),
         ],
         compiler_params=pltpu.CompilerParams(

time: 54 us -> 51.7 us (0.957)
  Pallas kernels: 53.3 us -> 50.9 us
    pallas_call x1, Pallas kernels: 51.9 us -> 49.5 us  [step(): pl.pallas_call(kernel, out_shape=(pltpu.VMEM((ROWS, PIECE), BF16), pltpu....]
where the time goes in v5:
time: 51.7 us; the launch traced here: 51.6 us
  Pallas kernels  50.9 us (98%)
  between operations  0.64 us (1%)
    pallas_call x1, Pallas kernels, step(): pl.pallas_call(kernel, out_shape=(pltpu.VMEM((ROWS, PIECE), BF16), pltpu....  49.5 us
    pallas_call x1, Pallas kernels, step(): pl.pallas_call(written_out, out_shape=tuple((jax.ShapeDtypeStruct(r.shape...  1.39 us

profile of v5, /device:TPU:1, one launch (start us, length us, event | category | flops | bytes accessed | tf_op | source)
XLA Modules:
  0.0 51.6 jit_solution(4536780376270722107)
XLA Ops:
  0.6 49.5 %decode_step.1 = (bf16[16,256]{1,0:T(8,128)(2,1)S(1)}, f32[16,256,128]{2,1,0:T(8,128)S(1)}) custom-call(bf16[16,4096]{1,0:T(8,128)(2,1)} %tok_h.1, bf16[256,1024]{1,0:T(8,128)(2,1)} %qw_h.1, bf16[256,1024]{1,0:T(8,128)(2,1)} %kw_h.1, bf16[4096,128]{1,0:T(8,128)(2,1)} %vw_h.1, bf16[16,4096]{1,0:T(8,128)(2,1)} %bitcast.10, f32[16,1024]{1,0:T(8,128)} %du_h.1, ...), custom_call_target="tpu_custom_call" | custom-call | tf_op jit(solution)/shard_map/decode_step/pallas_call | solution.py:409
  50.2 1.4 %written_out.1 = (bf16[16,256]{1,0:T(8,128)(2,1)}, f32[16,256,128]{2,1,0:T(8,128)}) custom-call(bf16[16,256]{1,0:T(8,128)(2,1)S(1)} %get-tuple-element.4.out, f32[16,256,128]{2,1,0:T(8,128)S(1)} %get-tuple-element.5.state), custom_call_target="tpu_custom_call" | custom-call | tf_op jit(solution)/shard_map/written_out/pallas_call | solution.py:441

commit v6 on v5

--- a/solution.py
+++ b/solution.py
@@ -26,6 +26,7 @@
 KEYS = 256
 LANES = 128
 FAR = (4, 3, 5, 2, 6, 1, 7)
+QUARTER = 1024
 ALL_TP = [(d, x) for d in FAR for x in (1, 0)] + [(0, 1)]
 ALL_EP = sorted(
     [(dy, dx) for dy in range(4) for dx in range(4) if dy or dx],
@@ -62,6 +63,12 @@
     )
 
 
+def thirds_of(x):
+    high = x.astype(BF16).astype(F32)
+    middle = (x - high).astype(BF16).astype(F32)
+    return [high, middle, (x - high - middle).astype(BF16).astype(F32)]
+
+
 def diagonal(offset):
     return iota((ROWS, LANES), 1) == iota((ROWS, LANES), 0) + offset
 
@@ -89,7 +96,7 @@
     tok_h, qw_h, kw_h, vw_h, dd_h, du_h, db_h, st_h, ow_h, ng_h, rw_h, rt_h, glu_h, lin_h, dn_h, fg_h,
     out_ref, ns,
     tok, qw, kw, vw, dd, du, db, st, ow, ng, rw, rt, gl, dn, fg, tok_part, decayed,
-    sq, rq, vals, val_out, mixed, sp, rp, rg, hid, nrm, sd, rd, su, ru, sr, rr, sm, rm, ss, rs, ns_in,
+    sq, rq, vals, val_out, mixed, sp, rp, sg, rg, hid, nrm, sd, rd, su, sb, rb, sr, rr, sm, rm, ss, rs, ns_in, lg,
     loc, out_sem, in_sem,
 ):
     e = lax.axis_index("ep")
@@ -105,6 +112,12 @@
     def ep_at(dy, dx):
         return 4 * lax.rem(e // 4 + dy, 4) + lax.rem(lax.rem(e, 4) + dx, 4)
 
+    def wide_piece(i):
+        return pl.ds(pl.multiple_of(i * 2 * PIECE, 2 * PIECE), 2 * PIECE)
+
+    def block(j, core):
+        return pl.ds(pl.multiple_of((2 * j + core) * PIECE, PIECE), PIECE)
+
     mark("fetch")
     units = pl.ds(pl.multiple_of(c * LANES, LANES), LANES)
     linear_units = pl.ds(pl.multiple_of((2 + c) * LANES, LANES), LANES)
@@ -115,23 +128,24 @@
     head_cols = pl.ds(pl.multiple_of(head * KEYS, KEYS), KEYS)
     fetches = [
         (tok_h, tok), (qw_h, qw), (kw_h, kw), (dd_h, dd), (du_h.at[:, head_cols], du), (db_h.at[:, head_cols], db),
-        (vw_h, vw), (st_h.at[rows_of(c)], st.at[c]), (ow_h, ow.at[units, :]), (ng_h, ng), (rw_h, rw), (rt_h, rt),
-        (fg_h.at[:, pl.ds(pl.multiple_of(t * PIECE, PIECE), PIECE)], fg),
-        (tok_h.at[rows_of(c), :], tok_part),
+        (vw_h, vw), (st_h.at[rows_of(c)], st.at[c]), (tok_h.at[rows_of(c), :], tok_part), (ow_h, ow.at[units, :]),
     ]
     copies = [pltpu.make_async_copy(a, b, loc.at[i]) for i, (a, b) in enumerate(fetches)]
     for copy in copies:
         copy.start()
+    own_cols = pl.ds(pl.multiple_of(t * PIECE, PIECE), PIECE)
+    later = [(ng_h, ng), (rw_h, rw), (rt_h, rt), (fg_h.at[:, own_cols], fg)]
+    late_copies = [pltpu.make_async_copy(a, b, loc.at[3 + i]) for i, (a, b) in enumerate(later)]
 
 
     def expert_weights(core):
-        blocks = [(glu_h.at[:, core], gl.at[:, :, units]), (lin_h.at[:, core], gl.at[:, :, linear_units])]
-        for j in range(N // 2):
-            cols = pl.ds(pl.multiple_of((2 * j + core) * PIECE, PIECE), PIECE)
-            blocks.append((dn_h.at[0, :, cols], dn.at[j, units, :]))
-        return blocks
-
-    own_weights = [pltpu.make_async_copy(a, b, loc.at[14 + i]) for i, (a, b) in enumerate(expert_weights(c))]
+        return [
+            (glu_h.at[:, core], gl.at[:, :, units]),
+            (lin_h.at[:, core], gl.at[:, :, linear_units]),
+            (dn_h.at[0], dn.at[units, :]),
+        ]
+
+    own_weights = [pltpu.make_async_copy(a, b, loc.at[i]) for i, (a, b) in enumerate(expert_weights(c))]
 
     def fetched(*which):
         for i in which:
@@ -182,7 +196,9 @@
     rq[t] = sq[c, head]
 
     mark("decay")
-    fetched(3, 4, 5, 6, 13)
+    fetched(3, 4, 5, 6, 8)
+    for copy in late_copies:
+        copy.start()
     values = dot(tok[...], vw[...]).astype(BF16).astype(F32)
     mine_first = c == 0
     val_out[...] = jnp.where(mine_first, values[PART:], values[:PART])
@@ -193,11 +209,7 @@
     pre = jnp.dot(low_rank, du[...], precision=lax.Precision.HIGHEST, preferred_element_type=F32) + db[...]
     log_sig = -(jnp.maximum(-pre, 0.0) + jnp.log1p(jnp.exp(-jnp.abs(pre))))
     decay = jnp.exp(log_sig / TAU)
-    hi = decay.astype(BF16)
-    rest = decay - hi.astype(F32)
-    mid = rest.astype(BF16)
-    low = (rest - mid.astype(F32)).astype(BF16)
-    thirds = jnp.concatenate([hi.astype(F32), mid.astype(F32), low.astype(F32)], axis=0)
+    thirds = jnp.concatenate(thirds_of(decay), axis=0)
     wide = PART * LANES
     ones3 = (lax.rem(iota((3 * PART, wide), 0), PART) == iota((3 * PART, wide), 1) // LANES).astype(BF16)
     decay_wide = dot(jnp.transpose(thirds).astype(BF16), ones3)
@@ -227,20 +239,22 @@
             mixed[s : s + 1, g * LANES : (g + 1) * LANES] = line
     match = jnp.sum(query * keys, axis=1, keepdims=True)
     mark("out_dot_s2")
-    fetched(8)
+    fetched(9)
     arrived(12, ow.at[pl.ds(0, LANES), :], None)
     readout = (mixed[...] + match * values_f) * KEYS ** (-0.5)
-    attn_part = dot(readout.astype(BF16), ow[...]).astype(BF16)
-    for i in range(N // 2):
-        sp[i] = attn_part[:, i * 2 * PIECE : (i + 1) * 2 * PIECE]
-    for d in FAR:
-        send(2, sp.at[lax.rem(z + d, N // 2)], rp.at[z], tp=tp_at(d, 0))
+    readout = readout.astype(BF16)
+    for steps in ((4,), (3, 5), (2, 6), (1, 7)):
+        for d in steps:
+            to = lax.rem(z + d, N // 2)
+            sp[to] = dot(readout, ow[:, wide_piece(to)]).astype(BF16)
+        for d in steps:
+            send(2, sp.at[lax.rem(z + d, N // 2)], rp.at[z], tp=tp_at(d, 0))
     sent(2, rp, N // 2 - 1)
-    rp[z] = sp[z]
+    rp[z] = dot(readout, ow[:, wide_piece(z)]).astype(BF16)
     for copy in own_weights:
         copy.start()
     for i, (mine, theirs) in enumerate(expert_weights(1 - c)):
-        send(min(13 + i, 15), mine, theirs, tp=partner)
+        send(13 + i, mine, theirs, tp=partner)
 
     mark("update")
     update = dot(jnp.transpose(keys).astype(BF16), values_wide)
@@ -249,7 +263,8 @@
             at = (g * PART + s) * LANES
             decayed[g, s] = decayed[g, s] + update[:, at : at + LANES]
     mark("slots")
-    fetched(9, 10, 11)
+    for copy in late_copies:
+        copy.wait()
     slots = N * CAP
     routed = rt[...]
     ids = iota((N, ROWS), 0)
@@ -264,77 +279,107 @@
     mark("r2_wait")
     arrived(2, rp, N // 2 - 1)
     mark("s3_send")
-    rg[t] = jnp.sum(rp[...].astype(F32), axis=0).astype(BF16)
-    for p in ALL_TP:
-        send(3, rg.at[t], rg.at[t], tp=tp_at(*p))
+    attn = jnp.sum(rp[...].astype(F32), axis=0).astype(BF16)
+    piece = ALPHA * tok_part[:, wide_piece(z)].astype(F32) + attn.astype(F32)
+    part_mean = jnp.mean(piece, axis=1, keepdims=True)
+    part_sq = jnp.sum((piece - part_mean) ** 2, axis=1, keepdims=True)
+    lane = iota((PART, LANES), 1)
+    stats = jnp.zeros((PART, LANES), F32)
+    for i, third in enumerate(thirds_of(part_mean) + thirds_of(part_sq)):
+        stats = jnp.where(lane == i, third, stats)
+    for i in range(2):
+        sg[i, :, :PIECE] = attn[:, i * PIECE : (i + 1) * PIECE]
+        sg[i, :, PIECE:] = stats.astype(BF16)
+    for d, x in ALL_TP:
+        to = tp_at(d, x)
+        send(3, sg.at[lax.rem(to, 2)], rg.at[t], tp=to)
+    rg[t] = sg[c]
     sent(3, rg, N - 1)
     send(10, decayed.at[1 - c], ns_in, tp=partner)
     sent(10, ns_in, None)
     for s in range(PART):
         ns[c * PART + s] = decayed[c, s]
+    rw_half = jnp.concatenate([rw[:, block(j, c)] for j in range(N // 2)], axis=1)
+    ng_half = jnp.concatenate([ng[:, block(j, c)] for j in range(N // 2)], axis=1)
+    for j in range(N // 2):
+        hid[:, j * PIECE : (j + 1) * PIECE] = ALPHA * tok[:, block(j, c)].astype(F32)
     mark("r3_wait")
     arrived(3, rg, N - 1)
 
     mark("norm1")
-    def block(j, core):
-        return pl.ds(pl.multiple_of((2 * j + core) * PIECE, PIECE), PIECE)
-
-    for i in range(N // 2):
-        cols = slice(i * 2 * PIECE, (i + 1) * 2 * PIECE)
-        attn = jnp.concatenate([rg[2 * i].astype(F32), rg[2 * i + 1].astype(F32)], axis=0)
-        hid[:, cols] = ALPHA * tok[:, cols].astype(F32) + attn
-    hidden = hid[...]
-    centred = hidden - jnp.mean(hidden, axis=1, keepdims=True)
-    var = jnp.mean(centred * centred, axis=1, keepdims=True)
-    nrm[...] = (centred * lax.rsqrt(var + EPSILON) * ng[...]).astype(BF16)
-
-    mark("s4_send")
-    half = jnp.concatenate([nrm[:, block(j, c)] for j in range(N // 2)], axis=1)
-    sd[...] = dot(spread.astype(BF16), half).astype(BF16).reshape(N, CAP, HALF)
-    for p in ALL_EP:
-        to = ep_at(*p)
-        send(4, sd.at[to], rd.at[e], ep=to)
-    sent(4, sd, N - 1)
-    rd[e] = sd[e]
+    stats = rg[:, :, PIECE:].reshape(N * PART, LANES).astype(F32)
+    lane = iota((N * PART, LANES), 1)
+
+    def by_chip(first):
+        column = jnp.sum(jnp.where((lane >= first) & (lane < first + 3), stats, 0.0), axis=1, keepdims=True)
+        return [column[i * ROWS : (i + 1) * ROWS] for i in range(N // 2)]
+
+    means, squares = by_chip(0), by_chip(3)
+    mean = sum(means) / (N // 2)
+    var = (sum(squares) + 2 * PIECE * sum((m - mean) ** 2 for m in means)) / D
+    scale = lax.rsqrt(var + EPSILON)
+    picked = spread.astype(BF16)
+    for a in range(2):
+        for j in range(4 * a, 4 * a + 4):
+            cols = slice(j * PIECE, (j + 1) * PIECE)
+            attn = jnp.concatenate([rg[2 * j, :, :PIECE].astype(F32), rg[2 * j + 1, :, :PIECE].astype(F32)], axis=0)
+            nrm[:, cols] = ((hid[:, cols] + attn - mean) * scale * ng_half[:, cols]).astype(BF16)
+
+        sd[a] = dot(picked, nrm[:, a * QUARTER : (a + 1) * QUARTER]).astype(BF16).reshape(N, CAP, QUARTER)
+        for p in ALL_EP:
+            to = ep_at(*p)
+            send(4 + 12 * a, sd.at[a, to], rd.at[a, e], ep=to)
+        sent(4 + 12 * a, sd.at[0], N - 1)
+        rd[a, e] = sd[a, e]
 
     mark("gates")
-    logits = dot_nt(rw[...], nrm[...])
+    logit_part = dot_nt(rw_half, nrm[...])
+    lg[c] = jnp.concatenate([logit_part, jnp.zeros((N, LANES - ROWS), F32)], axis=1)
+    send(7, lg.at[c], lg.at[c], tp=partner)
+    sent(7, lg, 1)
     arrived(10, ns_in, None)
     for s in range(PART):
         ns[(1 - c) * PART + s] = ns_in[s]
 
     mark("r4_wait_fwd")
-    arrived(4, rd, N - 1)
+    arrived(4, rd.at[0], N - 1)
     mark("up")
-    rows = rd[...].reshape(N * CAP, HALF)
     for copy in own_weights[:2]:
         copy.wait()
     arrived(13, gl.at[:, :, pl.ds(0, LANES)], None)
     arrived(14, gl.at[:, :, pl.ds(0, LANES)], None)
-    su[...] = dot(rows, gl[...].reshape(HALF, 4 * LANES))
-    send(5, su, ru, tp=partner)
-    sent(5, su, None)
+    first = dot(rd[0].reshape(N * CAP, QUARTER), gl[0:4].reshape(QUARTER, 4 * LANES))
+    mark("r4_wait2")
+    arrived(16, rd.at[1], N - 1)
+    mark("up2")
+    su[...] = first + dot(rd[1].reshape(N * CAP, QUARTER), gl[4:8].reshape(QUARTER, 4 * LANES))
+    sb[...] = su[...].astype(BF16)
+    send(5, sb, rb, tp=partner)
+    sent(5, sb, None)
     mark("up_wait")
-    arrived(5, ru, None)
+    arrived(5, rb, None)
     mark("down")
-    pre_act = su[...] + ru[...]
+    pre_act = su[...] + rb[...].astype(F32)
     glu = jnp.minimum(pre_act[:, : 2 * LANES], LIMIT)
     linear = jnp.clip(pre_act[:, 2 * LANES :], -LIMIT, LIMIT)
     act = (glu * jax.nn.sigmoid(SLOPE * glu) * (linear + 1.0)).astype(BF16)
 
     mark("down")
-    for copy in own_weights[2:]:
-        copy.wait()
-    arrived(15, dn.at[:, pl.ds(0, LANES), :], None)
-    for j in range(N // 2):
-        sr[:, :, j * PIECE : (j + 1) * PIECE] = dot(act, dn[j]).astype(BF16).reshape(N, CAP, PIECE)
-    mark("s6_send")
-    for p in ALL_EP:
-        to = ep_at(*p)
-        send(8, sr.at[to], rr.at[e], ep=to)
-    sent(8, sr, N - 1)
-    rr[e] = sr[e]
+    own_weights[2].wait()
+    arrived(15, dn.at[pl.ds(0, LANES), :], None)
+    order = FAR + (0,)
+    for a in range(2):
+        for i in range(4):
+            weights = dn[:, block(lax.rem(z + order[4 * a + i], N // 2), c)]
+            sr[a, :, :, i * PIECE : (i + 1) * PIECE] = dot(act, weights).astype(BF16).reshape(N, CAP, PIECE)
+        for p in ALL_EP:
+            to = ep_at(*p)
+            send(8 + 9 * a, sr.at[a, to], rr.at[a, e], ep=to)
+        sent(8 + 9 * a, sr.at[0], N - 1)
+        rr[a, e] = sr[a, e]
     mark("gates2")
+    arrived(7, lg, 1)
+    logits = (lg[0] + lg[1])[:, :ROWS]
     raised = jnp.where(chosen > 0.5, jnp.exp(logits), 0.0)
     gates = raised / jnp.sum(raised, axis=0, keepdims=True)
     gate_rows = spread * jnp.dot(
@@ -345,22 +390,29 @@
     gate_lo = (gate_cols - gate_hi.astype(F32)).astype(BF16)
 
     mark("r6_wait")
-    arrived(8, rr, N - 1)
+    arrived(8, rr.at[0], N - 1)
 
     mark("mix_s7")
-    back = rr[...].reshape(N * CAP, HALF)
-    mix = (dot(gate_hi, back) + dot(gate_lo, back)).astype(BF16)
-    for j in range(N // 2):
-        sm[j] = mix[:, j * PIECE : (j + 1) * PIECE]
-    for d in FAR:
-        to = lax.rem(z + d, N // 2)
-        send(9, sm.at[to], rm.at[z], tp=2 * to + c)
+    def mixed_piece(i):
+        back = rr[i // 4, :, :, (i % 4) * PIECE : (i % 4 + 1) * PIECE].reshape(N * CAP, PIECE)
+        return (dot(gate_hi, back) + dot(gate_lo, back)).astype(BF16)
+
+    for places in ((0,), (1, 2, 3), (4, 5, 6)):
+        if places[0] == 4:
+            mark("r6_wait2")
+            arrived(17, rr.at[1], N - 1)
+            mark("mix2")
+        for i in places:
+            sm[lax.rem(z + order[i], N // 2)] = mixed_piece(i)
+        for i in places:
+            to = lax.rem(z + order[i], N // 2)
+            send(9, sm.at[to], rm.at[z], tp=2 * to + c)
     sent(9, sm, N // 2 - 1)
-    rm[z] = sm[z]
+    rm[z] = mixed_piece(7)
     mark("r7_wait")
     arrived(9, rm, N // 2 - 1)
     mark("stats_s8")
-    own = nrm[:, pl.ds(pl.multiple_of(t * PIECE, PIECE), PIECE)].astype(F32)
+    own = nrm[:, pl.ds(pl.multiple_of(z * PIECE, PIECE), PIECE)].astype(F32)
     u = ALPHA * own + jnp.sum(rm[...].astype(F32), axis=0)
 
     ss[...] = moments(u)
@@ -369,7 +421,6 @@
     sent(6, rs, N - 1)
     rs[t] = ss[...]
     mark("r8_wait")
-    fetched(12)
     arrived(6, rs, N - 1)
     mark("final")
     mean, scale = merged(rs)
@@ -380,7 +431,7 @@
     sent(12, ow.at[pl.ds(0, LANES), :], None)
     sent(13, gl.at[:, :, pl.ds(0, LANES)], None)
     sent(14, gl.at[:, :, pl.ds(0, LANES)], None)
-    sent(15, dn.at[:, pl.ds(0, LANES), :], None)
+    sent(15, dn.at[pl.ds(0, LANES), :], None)
     for phase, like, count in pending:
         whole(phase, like, count).wait_send()
     mark(None)
@@ -418,15 +469,15 @@
             vmem((ROWS, D), BF16), vmem((PIECE, 1024), BF16), vmem((PIECE, 1024), BF16), vmem((D, LANES), BF16),
             vmem((N, D), BF16), vmem((16, KEYS), F32), vmem((1, KEYS), F32), vmem((2, PART, KEYS, LANES), F32),
             vmem((2 * LANES, D), BF16), vmem((1, D), F32), vmem((N, D), BF16), vmem((2, ROWS), jnp.int32),
-            vmem((N // 2, PIECE, 4 * LANES), BF16), vmem((N // 2, 2 * LANES, PIECE), BF16), vmem((1, PIECE), F32), vmem((PART, D), BF16), vmem((2, PART, KEYS, LANES), F32),
+            vmem((N // 2, PIECE, 4 * LANES), BF16), vmem((2 * LANES, D), BF16), vmem((1, PIECE), F32), vmem((PART, D), BF16), vmem((2, PART, KEYS, LANES), F32),
             vmem((2, 4, PART, 2 * KEYS), BF16), vmem((N, PART, 2 * KEYS), BF16), vmem((2, PART, LANES), F32),
             vmem((PART, LANES), F32), vmem((PART, 2 * LANES), F32), vmem((N // 2, PART, 2 * PIECE), BF16),
-            vmem((N // 2, PART, 2 * PIECE), BF16), vmem((N, PART, 2 * PIECE), BF16), vmem((ROWS, D), F32), vmem((ROWS, D), BF16),
-            vmem((N, CAP, HALF), BF16), vmem((N, CAP, HALF), BF16),
-            vmem((N * CAP, 4 * LANES), F32), vmem((N * CAP, 4 * LANES), F32),
-            vmem((N, CAP, HALF), BF16), vmem((N, CAP, HALF), BF16), vmem((N // 2, ROWS, PIECE), BF16),
-            vmem((N // 2, ROWS, PIECE), BF16), vmem((1, LANES), F32), vmem((N, 1, LANES), F32), vmem((PART, KEYS, LANES), F32),
-            dma((24,)), dma((16,)), dma((16,)),
+            vmem((N // 2, PART, 2 * PIECE), BF16), vmem((2, PART, PIECE + LANES), BF16), vmem((N, PART, PIECE + LANES), BF16), vmem((ROWS, HALF), F32), vmem((ROWS, HALF), BF16),
+            vmem((2, N, CAP, QUARTER), BF16), vmem((2, N, CAP, QUARTER), BF16),
+            vmem((N * CAP, 4 * LANES), F32), vmem((N * CAP, 4 * LANES), BF16), vmem((N * CAP, 4 * LANES), BF16),
+            vmem((2, N, CAP, QUARTER), BF16), vmem((2, N, CAP, QUARTER), BF16), vmem((N // 2, ROWS, PIECE), BF16),
+            vmem((N // 2, ROWS, PIECE), BF16), vmem((1, LANES), F32), vmem((N, 1, LANES), F32), vmem((PART, KEYS, LANES), F32), vmem((2, N, LANES), F32),
+            dma((10,)), dma((18,)), dma((18,)),
         ],
         compiler_params=pltpu.CompilerParams(
             collective_id=0, has_side_effects=True, vmem_limit_bytes=60 * 1024 * 1024

time: 51.7 us -> 50.1 us (0.969)
  Pallas kernels: 50.9 us -> 49.4 us
    pallas_call x1, Pallas kernels: 49.5 us -> 48 us  [step(): pl.pallas_call(kernel, out_shape=(pltpu.VMEM((ROWS, PIECE), BF16), pltpu....]
where the time goes in v6:
time: 50.1 us; the launch traced here: 50 us
  Pallas kernels  49.4 us (99%)
  between operations  0.64 us (1%)
    pallas_call x1, Pallas kernels, step(): pl.pallas_call(kernel, out_shape=(pltpu.VMEM((ROWS, PIECE), BF16), pltpu....  48 us
    pallas_call x1, Pallas kernels, step(): pl.pallas_call(written_out, out_shape=tuple((jax.ShapeDtypeStruct(r.shape...  1.39 us

profile of v6, /device:TPU:1, one launch (start us, length us, event | category | flops | bytes accessed | tf_op | source)
XLA Modules:
  0.0 50.0 jit_solution(9770010570323906290)
XLA Ops:
  0.6 48.0 %decode_step.1 = (bf16[16,256]{1,0:T(8,128)(2,1)S(1)}, f32[16,256,128]{2,1,0:T(8,128)S(1)}) custom-call(bf16[16,4096]{1,0:T(8,128)(2,1)} %tok_h.1, bf16[256,1024]{1,0:T(8,128)(2,1)} %qw_h.1, bf16[256,1024]{1,0:T(8,128)(2,1)} %kw_h.1, bf16[4096,128]{1,0:T(8,128)(2,1)} %vw_h.1, bf16[16,4096]{1,0:T(8,128)(2,1)} %bitcast.10, f32[16,1024]{1,0:T(8,128)} %du_h.1, ...), custom_call_target="tpu_custom_call" | custom-call | tf_op jit(solution)/shard_map/decode_step/pallas_call | solution.py:460
  48.6 1.4 %written_out.1 = (bf16[16,256]{1,0:T(8,128)(2,1)}, f32[16,256,128]{2,1,0:T(8,128)}) custom-call(bf16[16,256]{1,0:T(8,128)(2,1)S(1)} %get-tuple-element.4.out, f32[16,256,128]{2,1,0:T(8,128)S(1)} %get-tuple-element.5.state), custom_call_target="tpu_custom_call" | custom-call | tf_op jit(solution)/shard_map/written_out/pallas_call | solution.py:492
